TPU v7x, 32 devices: a whole 2x2x4 slice. The times are simulated.
32 devices in a mesh: sp: 8 (over z, x), tp: 4 (over y, core).
Axes of the slice: x: 2, y: 2, z: 4, core: 2. Of those that a mesh axis runs over, the one named last changes fastest.
Arguments:
- glu_value: bfloat16 [1024, 2048], P('tp', 'sp')
- glu_gate: bfloat16 [1024, 2048], P('tp', 'sp'), may hold values from -8 to 8
- conv_taps: float32 [1024, 31], P('tp'), may hold values from -1 to 1
- norm_gain: float32 [1024], P('tp'), may hold values from 0.1 to 1.9
- out_proj: bfloat16 [1024, 2048], P(None, 'tp'), may hold values from -0.1875 to 0.1875
- resid: bfloat16 [2048, 2048], P('sp', 'tp'), may hold values from -6 to 6
- expert_ids: int32 [2048, 2], P('sp'), may hold values from 0 to 7, all different within a row; in each aligned block of 256 rows (0 to 255, 256 to 511, ...) at most 128 rows name the same one
- route_logits: float32 [2048, 2], P('sp'), may hold values from -8 to 8
- group_prob: float32 [2048], P('sp'), may hold values from 0.2 to 1
- w_gate: bfloat16 [8, 2048, 4096], P('sp', None, 'tp'), may hold values from -0.125 to 0.125
- w_up: bfloat16 [8, 2048, 4096], P('sp', None, 'tp'), may hold values from -0.125 to 0.125
- w_down: bfloat16 [8, 4096, 2048], P('sp', None, 'tp'), may hold values from -0.09375 to 0.09375
Outputs:
- layer_out: bfloat16 [2048, 2048], P('sp', 'tp')
Inputs may be any that keep to these rules, and one draw needn't show every extreme that they name: `expert_ids`: each row names 2 different experts. In each aligned block of 256 rows (the rows of one index of sp) no expert is named by more than 128 rows, a bound that some block reaches.
All inputs are finite; a program needn't handle non-finite values.
Results may differ from a plain program's by a relative error of at most 0.0061.
Values may be sent and summed in bfloat16 or wider, within the bound.
A program may use at most 64 MiB of HBM per device.

v0:
```python
import functools

import jax
import jax.numpy as jnp
from jax import lax
from jax.experimental import pallas as pl
from jax.experimental.pallas import tpu as pltpu
from jax.sharding import PartitionSpec as P

MESH = pl.DeviceIdType.MESH


def expert_kernel(
    n_sp,
    n_tp,
    filtered,
    gain,
    proj,
    resid,
    id_rows,
    id_cols,
    logits,
    prob,
    w_gate,
    w_up,
    w_down,
    out,
    stats,
    act,
    mixed,
    slots,
    route,
    total,
    outgoing,
    rows,
    hidden,
    results,
    returned,
    gate_v,
    up_v,
    down_v,
    load_sem,
    own_sem,
    stat_send,
    stat_recv,
    act_recv,
    act_far,
    act_near,
    out_send,
    rows_recv,
    rows_far,
    rows_near,
    hid_recv,
    hid_far,
    hid_near,
    ret_send,
    ret_recv,
):
    e = lax.axis_index("sp")
    q = lax.axis_index("tp")
    n_y = n_tp // 2
    y, core = q // 2, q % 2
    sibling = 2 * y + (1 - core)
    _, capacity, width = results.shape
    tokens = mixed.shape[0]
    ff_local = gate_v.shape[1]

    def source(k):
        if n_sp & (n_sp - 1) or n_sp == 1:
            return lax.rem(e + k, n_sp)
        k = jnp.where(k == 0, 0, lax.rem(k, n_sp - 1) + 1) if n_sp > 2 else k
        at, bit = 0, 1
        while bit < n_sp:
            at, bit = at + (e // bit + k // bit) % 2 * bit, 2 * bit
        return at

    def target(k):
        if n_sp & (n_sp - 1) or n_sp == 1:
            return lax.rem(e + n_sp - k, n_sp)
        return source(k)

    def rows_at(s, t):
        return rows.at[s, :, pl.ds(pl.multiple_of(t * width, width), width)]

    def act_at(s, t):
        return act.at[t]

    def hidden_at(s, t):
        return hidden.at[s, :, pl.ds(pl.multiple_of(t * ff_local, ff_local), ff_local)]

    def far(j):
        return 2 * lax.rem(y + j, n_y) + core

    def behind(j):
        return 2 * lax.rem(y + n_y - j, n_y) + core

    def share(at, recv, s, t, send, peer):
        return pltpu.make_async_remote_copy(
            src_ref=at(s, t),
            dst_ref=at(s, t),
            send_sem=send,
            recv_sem=recv.at[s, t],
            device_id=(e, peer),
            device_id_type=MESH,
        )

    def dispatch(k):
        to = target(k)
        return pltpu.make_async_remote_copy(
            src_ref=outgoing.at[to],
            dst_ref=rows_at(e, q),
            send_sem=out_send.at[k],
            recv_sem=rows_recv.at[e, q],
            device_id=(to, q),
            device_id_type=MESH,
        )

    def give_back(k):
        s = source(k)
        return pltpu.make_async_remote_copy(
            src_ref=results.at[s],
            dst_ref=returned.at[e],
            send_sem=ret_send.at[k],
            recv_sem=ret_recv.at[e],
            device_id=(s, q),
            device_id_type=MESH,
        )

    def arrived(at, recv, s, t):
        pltpu.make_async_copy(at(s, t), at(s, t), recv.at[s, t]).wait()

    def tell(o):
        return pltpu.make_async_remote_copy(
            src_ref=stats.at[q],
            dst_ref=stats.at[q],
            send_sem=stat_send.at[o],
            recv_sem=stat_recv.at[q],
            device_id=(e, lax.rem(q + o, n_tp)),
            device_id_type=MESH,
        )

    loads = [
        pltpu.make_async_copy(w_gate.at[0], gate_v, load_sem.at[0]),
        pltpu.make_async_copy(w_up.at[0], up_v, load_sem.at[1]),
        pltpu.make_async_copy(w_down.at[0], down_v, load_sem.at[2]),
    ]
    barrier = pltpu.get_barrier_semaphore()

    @pl.loop(1, n_sp)
    def _(k):
        pl.semaphore_signal(barrier, inc=1, device_id=(source(k), q), device_id_type=MESH)

    for o in range(1, n_tp):
        pl.semaphore_signal(
            barrier, inc=1, device_id=(e, lax.rem(q + o, n_tp)), device_id_type=MESH
        )
    for load in loads:
        load.start()

    top = id_rows.shape[0]
    ahead = lax.broadcasted_iota(jnp.int32, (tokens, tokens), 0)
    after = lax.broadcasted_iota(jnp.int32, (tokens, tokens), 1)
    lanes = max(128, n_sp)
    row_no = lax.broadcasted_iota(jnp.int32, (lanes, tokens), 0)
    col_no = lax.broadcasted_iota(jnp.int32, (tokens, lanes), 1)
    row_hit = [jnp.where(row_no == id_rows[r : r + 1], 1.0, 0.0) for r in range(top)]
    col_hit = [jnp.where(col_no == id_cols[:, r : r + 1], 1.0, 0.0) for r in range(top)]
    row_rank = jnp.dot(
        sum(row_hit).astype(jnp.bfloat16),
        jnp.where(ahead < after, 1.0, 0.0).astype(jnp.bfloat16),
        preferred_element_type=jnp.float32,
    )
    col_rank = jnp.dot(
        jnp.where(ahead > after, 1.0, 0.0).astype(jnp.bfloat16),
        sum(col_hit).astype(jnp.bfloat16),
        preferred_element_type=jnp.float32,
    )
    slot_rows = [
        (id_rows[r : r + 1] * capacity).astype(jnp.float32)
        + jnp.sum(row_hit[r] * row_rank, axis=0, keepdims=True)
        for r in range(top)
    ]
    for r in range(top):
        slots[:, r : r + 1] = (id_cols[:, r : r + 1] * capacity).astype(jnp.float32) + jnp.sum(
            col_hit[r] * col_rank, axis=1, keepdims=True
        )
    scores = logits[...]
    scores = jnp.exp(scores - jnp.max(scores, axis=1, keepdims=True))
    route[...] = prob[...] * scores / jnp.sum(scores, axis=1, keepdims=True)
    raw = filtered[...]
    stats[q, 0:1] = jnp.sum(raw, axis=0, keepdims=True)
    stats[q, 1:2] = jnp.sum(raw * raw, axis=0, keepdims=True)
    pl.semaphore_wait(barrier, n_sp - 1 + n_tp - 1)

    def spread(at, recv, far_sem, near_sem, s):
        for j in range(1, n_y):
            share(at, recv, s, q, far_sem.at[s, j], far(j)).start()
        share(at, recv, s, q, near_sem.at[s, 0], sibling).start()

    def relay(at, recv, near_sem, s):
        for j in range(1, n_y):
            t = behind(j)
            arrived(at, recv, s, t)
            share(at, recv, s, t, near_sem.at[s, j], sibling).start()

    def collect(at, recv, s):
        for j in range(n_y):
            arrived(at, recv, s, 2 * lax.rem(y + n_y - j, n_y) + (1 - core))

    def drain(at, recv, far_sem, near_sem, s):
        for j in range(1, n_y):
            share(at, recv, s, q, far_sem.at[s, j], far(j)).wait_send()
        share(at, recv, s, q, near_sem.at[s, 0], sibling).wait_send()
        for j in range(1, n_y):
            share(at, recv, s, behind(j), near_sem.at[s, j], sibling).wait_send()

    for o in range(1, n_tp):
        tell(o).start()
    for o in range(1, n_tp):
        t = lax.rem(q + o, n_tp)
        pltpu.make_async_copy(stats.at[t], stats.at[t], stat_recv.at[t]).wait()
    one = stats[0, 0:1]
    two = stats[0, 1:2]
    for t in range(1, n_tp):
        one = one + stats[t, 0:1]
        two = two + stats[t, 1:2]
    channels = proj.shape[0]
    mean = one / channels
    var = two / channels - mean * mean
    normed = (filtered[...] - mean) * lax.rsqrt(var + 1e-05) * gain[...]
    act[q] = (normed / (1.0 + jnp.exp(-normed))).astype(act.dtype)
    spread(act_at, act_recv, act_far, act_near, 0)
    relay(act_at, act_recv, act_near, 0)
    collect(act_at, act_recv, 0)
    depth = act.shape[1]
    sums = resid[...].astype(jnp.float32)
    for t in range(n_tp):
        sums = sums + lax.dot_general(
            act[t],
            proj[t * depth : (t + 1) * depth],
            (((0,), (0,)), ((), ())),
            preferred_element_type=jnp.float32,
        )
    mixed[...] = sums.astype(mixed.dtype)

    @pl.loop(0, n_sp)
    def _(k):
        to = target(k)
        place = (to * capacity + lax.broadcasted_iota(jnp.int32, (capacity, tokens), 0)).astype(
            jnp.float32
        )
        picks = jnp.zeros((capacity, tokens), jnp.float32)
        for r in range(top):
            picks = picks + jnp.where(place == slot_rows[r], 1.0, 0.0)
        outgoing[to] = jnp.dot(
            picks.astype(mixed.dtype), mixed[...], preferred_element_type=jnp.float32
        ).astype(outgoing.dtype)

        @pl.when(k > 0)
        def _():
            dispatch(k).start()

    total[...] = jnp.zeros_like(total)
    own_in = pltpu.make_async_copy(outgoing.at[e], rows_at(e, q), own_sem.at[0])
    own_in.start()

    def combine(x):
        place = (x * capacity + lax.broadcasted_iota(jnp.int32, (tokens, capacity), 1)).astype(
            jnp.float32
        )
        for r in range(top):
            picks = jnp.where(place == slots[:, r : r + 1], 1.0, 0.0).astype(mixed.dtype)
            got = jnp.dot(picks, returned[x], preferred_element_type=jnp.float32)
            total[...] += route[:, r : r + 1] * got

    tile = min(256, ff_local)
    out_tile = min(256, width)

    def up_step(s):
        @pl.loop(0, ff_local // tile)
        def _(i):
            at = pl.ds(pl.multiple_of(i * tile, tile), tile)
            g = jnp.dot(rows[s], gate_v[:, at], preferred_element_type=jnp.float32)
            u = jnp.dot(rows[s], up_v[:, at], preferred_element_type=jnp.float32)
            h = (g / (1.0 + jnp.exp(-g)) * u).astype(hidden.dtype)
            hidden[s, :, pl.ds(pl.multiple_of(q * ff_local + i * tile, tile), tile)] = h

    def down_step(s):
        @pl.loop(0, width // out_tile)
        def _(i):
            at = pl.ds(pl.multiple_of(i * out_tile, out_tile), out_tile)
            o = jnp.dot(hidden[s], down_v[:, at], preferred_element_type=jnp.float32)
            results[s, :, at] = o.astype(results.dtype)

    @pl.loop(0, n_sp + 4)
    def _(i):
        @pl.when(i < n_sp)
        def _():
            @pl.when(i == 0)
            def _():
                own_in.wait()

            @pl.when(i > 0)
            def _():
                arrived(rows_at, rows_recv, source(i), q)

            spread(rows_at, rows_recv, rows_far, rows_near, source(i))

        @pl.when((i >= 1) & (i < n_sp + 1))
        def _():
            relay(rows_at, rows_recv, rows_near, source(i - 1))

        @pl.when((i >= 2) & (i < n_sp + 2))
        def _():
            s = source(i - 2)
            collect(rows_at, rows_recv, s)

            @pl.when(i == 2)
            def _():
                for load in loads:
                    load.wait()

            up_step(s)
            spread(hidden_at, hid_recv, hid_far, hid_near, s)

        @pl.when((i >= 3) & (i < n_sp + 3))
        def _():
            relay(hidden_at, hid_recv, hid_near, source(i - 3))

        @pl.when(i >= 4)
        def _():
            s = source(i - 4)
            collect(hidden_at, hid_recv, s)
            down_step(s)

            @pl.when(i == 4)
            def _():
                pltpu.make_async_copy(results.at[e], returned.at[e], own_sem.at[1]).start()

            @pl.when(i > 4)
            def _():
                give_back(i - 4).start()

    pltpu.make_async_copy(results.at[e], returned.at[e], own_sem.at[1]).wait()
    combine(e)

    @pl.loop(1, n_sp)
    def _(k):
        x = target(k)
        pltpu.make_async_copy(returned.at[x], returned.at[x], ret_recv.at[x]).wait()
        combine(x)

    out[...] = (mixed[...].astype(jnp.float32) + total[...]).astype(out.dtype)

    for o in range(1, n_tp):
        tell(o).wait_send()
    drain(act_at, act_recv, act_far, act_near, 0)

    @pl.loop(0, n_sp)
    def _(s):
        drain(rows_at, rows_recv, rows_far, rows_near, s)
        drain(hidden_at, hid_recv, hid_far, hid_near, s)

    @pl.loop(1, n_sp)
    def _(k):
        dispatch(k).wait_send()
        give_back(k).wait_send()


def run_layer(filtered, gain, proj, resid, id_rows, id_cols, logits, prob, w_gate, w_up, w_down):
    n_sp, n_tp = lax.axis_size("sp"), lax.axis_size("tp")
    n_y = n_tp // 2
    tokens, width = resid.shape
    capacity = 4 * tokens // n_sp
    ff_local = w_gate.shape[2]
    dma = pltpu.SemaphoreType.DMA
    vmem = pl.BlockSpec(memory_space=pltpu.VMEM)
    return pl.pallas_call(
        functools.partial(expert_kernel, n_sp, n_tp),
        out_shape=jax.ShapeDtypeStruct(resid.shape, resid.dtype),
        in_specs=[vmem] * 8 + [pl.BlockSpec(memory_space=pl.ANY)] * 3,
        out_specs=vmem,
        scratch_shapes=[
            pltpu.VMEM((n_tp, 8, tokens), jnp.float32),
            pltpu.VMEM((n_tp,) + filtered.shape, jnp.bfloat16),
            pltpu.VMEM((tokens, width), jnp.bfloat16),
            pltpu.VMEM((tokens, id_cols.shape[1]), jnp.float32),
            pltpu.VMEM((tokens, id_cols.shape[1]), jnp.float32),
            pltpu.VMEM((tokens, width), jnp.float32),
            pltpu.VMEM((n_sp, capacity, width), jnp.bfloat16),
            pltpu.VMEM((n_sp, capacity, width * n_tp), jnp.bfloat16),
            pltpu.VMEM((n_sp, capacity, ff_local * n_tp), jnp.bfloat16),
            pltpu.VMEM((n_sp, capacity, width), jnp.bfloat16),
            pltpu.VMEM((n_sp, capacity, width), jnp.bfloat16),
            pltpu.VMEM(w_gate.shape[1:], jnp.bfloat16),
            pltpu.VMEM(w_up.shape[1:], jnp.bfloat16),
            pltpu.VMEM(w_down.shape[1:], jnp.bfloat16),
            dma((3,)),
            dma((2,)),
            dma((n_tp,)),
            dma((n_tp,)),
            dma((1, n_tp)),
            dma((1, n_y)),
            dma((1, n_y)),
            dma((n_sp,)),
            dma((n_sp, n_tp)),
            dma((n_sp, n_y)),
            dma((n_sp, n_y)),
            dma((n_sp, n_tp)),
            dma((n_sp, n_y)),
            dma((n_sp, n_y)),
            dma((n_sp,)),
            dma((n_sp,)),
        ],
        compiler_params=pltpu.CompilerParams(
            collective_id=0, has_side_effects=True, vmem_limit_bytes=52 * 1024 * 1024
        ),
    )(filtered, gain, proj, resid, id_rows, id_cols, logits, prob, w_gate, w_up, w_down)


def from_behind(block, axis, distance):
    devices = range(lax.axis_size(axis))
    route = [(i - distance, i) for i in devices if i - distance in devices]
    return lax.ppermute(block, axis, route)


def per_device(
    glu_value,
    glu_gate,
    conv_taps,
    norm_gain,
    out_proj,
    resid,
    expert_ids,
    route_logits,
    group_prob,
    w_gate,
    w_up,
    w_down,
):
    local_tokens = glu_value.shape[1]
    tap_count = conv_taps.shape[1]
    gated = (glu_value.astype(jnp.float32) * jax.nn.sigmoid(glu_gate.astype(jnp.float32))).astype(
        jnp.bfloat16
    )
    history = from_behind(gated[:, local_tokens - (tap_count - 1) :], "sp", 1)
    padded = jnp.concatenate([history, gated], axis=1).astype(jnp.float32)
    filtered = jnp.zeros(gated.shape, jnp.float32)
    for offset in range(tap_count):
        filtered = (
            filtered + conv_taps[:, offset : offset + 1] * padded[:, offset : offset + local_tokens]
        )
    return run_layer(
        filtered,
        norm_gain[:, None],
        out_proj,
        resid,
        expert_ids.T,
        expert_ids,
        route_logits,
        group_prob[:, None],
        w_gate,
        w_up,
        w_down,
    )


def solution(mesh):
    return jax.shard_map(
        per_device,
        mesh=mesh,
        in_specs=(
            P("tp", "sp"),
            P("tp", "sp"),
            P("tp", None),
            P("tp"),
            P(None, "tp"),
            P("sp", "tp"),
            P("sp", None),
            P("sp", None),
            P("sp"),
            P("sp", None, "tp"),
            P("sp", None, "tp"),
            P("sp", None, "tp"),
        ),
        out_specs=P("sp", "tp"),
        check_vma=False,
    )
```

profile of v0, /device:TPU:0, one launch (start us, length us, event | category | flops | bytes accessed | tf_op | source)
XLA Modules:
  0.0 118.9 jit_solution(7813659962865289738)
XLA Ops:
  0.0 1.0 multiply_convert_fusion
  1.0 0.1 slice.252
  1.1 4.9 %collective-permute-start = (bf16[256,30]{1,0:T(8,128)(2,1)S(1)}, bf16[256,30]{1,0:T(8,128)(2,1)S(1)}, u32[]{:S(2)}, u32[]{:S(2)}) collective-permute-start(bf16[256,30]{1,0:T(8,128)(2,1)S(1)} %slice.252), channel_id=1, source_target_pairs={{0,4},{4,8},{8,12},{12,16},{16,20},{20,24},{24,28},{1,5},{5,9},{9,... | collective-permute-start | bytes 46088 | tf_op jit(solution)/shard_map/ppermute | solution.py:424
  6.0 1.0 fusion.30
  7.0 1.0 fusion.31
  8.0 0.8 copy.15.gain
  8.8 0.8 copy.16.id_cols
  9.7 0.8 copy.17.logits
  10.5 0.8 copy.18.prob
  11.3 0.0 collective-permute-done
  11.3 0.1 maximum_convert_fusion
  11.4 0.0 copy-start
  11.5 0.0 copy-start.1
  11.5 3.5 %fusion.filtered = f32[256,256]{1,0:T(8,128)S(1)} fusion(f32[256,286]{1,0:T(8,128)S(1)} %maximum_convert_fusion, f32[256]{0:T(256)S(1)} %bitcast.64, f32[256]{0:T(256)S(1)} %bitcast.65, f32[256]{0:T(256)S(1)} %bitcast.36, f32[256]{0:T(256)S(1)} %bitcast.37, f32[256]{0:T(256)S(1)} %bitcast.38, f32[256]{0:T(256)S(1)} %bitcast.39, f32[256]{0:T(256)S(1)} %bitcast.40, ...), kind=kLoop, calls=%fused_computation.1 | loop fusion | flops 3997696 | bytes 8420352 | tf_op jit(solution)/shard_map/add | solution.py:451
  15.0 0.0 copy-done
  15.0 0.0 copy-done.1
  15.0 103.1 %shard_map.118 = bf16[256,512]{1,0:T(8,128)(2,1)S(1)} custom-call(f32[256,256]{1,0:T(8,128)S(1)} %fusion.filtered, f32[256,1]{1,0:T(8,128)S(1)} %copy.15.gain, bf16[1024,512]{1,0:T(8,128)(2,1)} %proj.1, bf16[256,512]{1,0:T(8,128)(2,1)S(1)} %copy-done, s32[2,256]{1,0:T(2,128)S(1)} %bitcast.34, s32[256,2]{1,0:T(8,128)S(1)} %copy.16.id_cols, ...), custom_call_target="tpu_custom_call" | custom-call | tf_op jit(solution)/shard_map/pallas_call | solution.py:378
  118.2 0.7 copy.20
Async XLA Ops:
  1.1 10.2 %collective-permute-start = (bf16[256,30]{1,0:T(8,128)(2,1)S(1)}, bf16[256,30]{1,0:T(8,128)(2,1)S(1)}, u32[]{:S(2)}, u32[]{:S(2)}) collective-permute-start(bf16[256,30]{1,0:T(8,128)(2,1)S(1)} %slice.252), channel_id=1, source_target_pairs={{0,4},{4,8},{8,12},{12,16},{16,20},{20,24},{24,28},{1,5},{5,9},{9,... | collective-permute-start | bytes 46088 | tf_op jit(solution)/shard_map/ppermute | solution.py:424
  11.4 3.5 %copy-start = (bf16[256,512]{1,0:T(8,128)(2,1)S(1)}, bf16[256,512]{1,0:T(8,128)(2,1)}, u32[]{:S(2)}) copy-start(bf16[256,512]{1,0:T(8,128)(2,1)} %resid.1) | copy-start | bytes 786436
  11.5 3.5 %copy-start.1 = (s32[256,2]{0,1:T(2,128)S(1)}, s32[256,2]{0,1:T(2,128)}, u32[]{:S(2)}) copy-start(s32[256,2]{0,1:T(2,128)} %param.18) | copy-start | bytes 6148
where the time goes:
time: 119 us
  Pallas kernels  103 us (87%)
  local copies, waits for them, and re-layouts  6.05 us (5%)
  starting transfers between devices  4.87 us (4%)
  other arithmetic  4.68 us (4%)
    pallas_call x1, Pallas kernels, run_layer(): pl.pallas_call(functools.partial(expert_kernel, n_sp, n_tp), out_shape=ja...  103 us
    ppermute x1, starting transfers between devices, from_behind(): return lax.ppermute(block, axis, route)  4.87 us
    add x1, other arithmetic, per_device(): filtered + conv_taps[:, offset:offset + 1] * padded[:, offset:offset + lo...  3.51 us
  transfers between devices with their start and end apart: 1, of which 0 were waited for; matrix products, arithmetic and copies ran while one was open for 4% of the time, Pallas kernels for 0%

commit v1 on v0

--- a/solution.py
+++ b/solution.py
@@ -13,23 +13,31 @@
 def expert_kernel(
     n_sp,
     n_tp,
-    filtered,
+    value,
+    gate,
+    taps,
     gain,
     proj,
     resid,
-    id_rows,
-    id_cols,
+    ids,
     logits,
     prob,
     w_gate,
     w_up,
     w_down,
     out,
+    padded,
+    sums,
+    halo_out,
+    halo_in,
+    gains,
     stats,
+    flip,
+    columns,
     act,
+    normal,
     mixed,
     slots,
-    route,
     total,
     outgoing,
     rows,
@@ -41,8 +49,13 @@
     down_v,
     load_sem,
     own_sem,
+    halo_sem,
+    gain_send,
+    gain_recv,
     stat_send,
     stat_recv,
+    head_send,
+    head_recv,
     act_recv,
     act_far,
     act_near,
@@ -64,6 +77,8 @@
     _, capacity, width = results.shape
     tokens = mixed.shape[0]
     ff_local = gate_v.shape[1]
+    history, local = halo_in.shape
+    taken = taps.shape[0]
 
     def source(k):
         if n_sp & (n_sp - 1) or n_sp == 1:
@@ -83,7 +98,10 @@
         return rows.at[s, :, pl.ds(pl.multiple_of(t * width, width), width)]
 
     def act_at(s, t):
-        return act.at[t]
+        return act.at[t, pl.ds(history, tokens - history)]
+
+    def head_at(t):
+        return act.at[t, pl.ds(0, history)]
 
     def hidden_at(s, t):
         return hidden.at[s, :, pl.ds(pl.multiple_of(t * ff_local, ff_local), ff_local)]
@@ -129,13 +147,35 @@
     def arrived(at, recv, s, t):
         pltpu.make_async_copy(at(s, t), at(s, t), recv.at[s, t]).wait()
 
-    def tell(o):
+    def tell(o, source, target, send, recv):
         return pltpu.make_async_remote_copy(
-            src_ref=stats.at[q],
-            dst_ref=stats.at[q],
-            send_sem=stat_send.at[o],
-            recv_sem=stat_recv.at[q],
+            src_ref=source,
+            dst_ref=target,
+            send_sem=send.at[o],
+            recv_sem=recv.at[q],
             device_id=(e, lax.rem(q + o, n_tp)),
+            device_id_type=MESH,
+        )
+
+    def tell_gain(o):
+        return tell(o, gain, gains.at[q], gain_send, gain_recv)
+
+    def tell_stats(o):
+        return tell(o, stats.at[q], stats.at[q], stat_send, stat_recv)
+
+    def tell_head(o):
+        return tell(o, head_at(q), head_at(q), head_send, head_recv)
+
+    def heard(ref, recv, t):
+        pltpu.make_async_copy(ref, ref, recv.at[t]).wait()
+
+    def hand_on():
+        return pltpu.make_async_remote_copy(
+            src_ref=halo_out,
+            dst_ref=halo_in,
+            send_sem=halo_sem.at[0],
+            recv_sem=halo_sem.at[1],
+            device_id=(lax.rem(e + 1, n_sp), q),
             device_id_type=MESH,
         )
 
@@ -157,39 +197,51 @@
     for load in loads:
         load.start()
 
-    top = id_rows.shape[0]
+    flow = value[...].astype(jnp.float32) / (1.0 + jnp.exp(-gate[...].astype(jnp.float32)))
+    flow = jnp.transpose(flow).astype(jnp.bfloat16)
+    halo_out[...] = flow[tokens - history :]
+    padded[history:] = flow.astype(jnp.float32)
+    lane = lax.broadcasted_iota(jnp.int32, (history, 128), 1)
+
+    def convolve(first):
+        filtered = jnp.zeros((history, local), jnp.float32)
+        for j in range(taken):
+            at = first + history - (taken - 1) + j
+            filtered = filtered + taps[j : j + 1] * padded[at : at + history]
+        one = jnp.sum(filtered, axis=1, keepdims=True)
+        two = jnp.sum(filtered * filtered, axis=1, keepdims=True)
+        sums[first : first + history] = jnp.where(lane == 0, one, jnp.where(lane == 1, two, 0.0))
+        act[q, first : first + history] = (filtered - one / local).astype(act.dtype)
+
+    for first in range(history, tokens, history):
+        convolve(first)
+    gains[q] = gain[...]
+
+    top = ids.shape[0]
     ahead = lax.broadcasted_iota(jnp.int32, (tokens, tokens), 0)
     after = lax.broadcasted_iota(jnp.int32, (tokens, tokens), 1)
     lanes = max(128, n_sp)
     row_no = lax.broadcasted_iota(jnp.int32, (lanes, tokens), 0)
-    col_no = lax.broadcasted_iota(jnp.int32, (tokens, lanes), 1)
-    row_hit = [jnp.where(row_no == id_rows[r : r + 1], 1.0, 0.0) for r in range(top)]
-    col_hit = [jnp.where(col_no == id_cols[:, r : r + 1], 1.0, 0.0) for r in range(top)]
+    row_hit = [jnp.where(row_no == ids[r : r + 1], 1.0, 0.0) for r in range(top)]
     row_rank = jnp.dot(
         sum(row_hit).astype(jnp.bfloat16),
         jnp.where(ahead < after, 1.0, 0.0).astype(jnp.bfloat16),
         preferred_element_type=jnp.float32,
     )
-    col_rank = jnp.dot(
-        jnp.where(ahead > after, 1.0, 0.0).astype(jnp.bfloat16),
-        sum(col_hit).astype(jnp.bfloat16),
-        preferred_element_type=jnp.float32,
-    )
     slot_rows = [
-        (id_rows[r : r + 1] * capacity).astype(jnp.float32)
+        (ids[r : r + 1] * capacity).astype(jnp.float32)
         + jnp.sum(row_hit[r] * row_rank, axis=0, keepdims=True)
         for r in range(top)
     ]
+    scores = logits[...]
+    scores = jnp.exp(scores - jnp.max(scores, axis=0, keepdims=True))
+    scores = prob[...] * scores / jnp.sum(scores, axis=0, keepdims=True)
+    flip[...] = jnp.zeros_like(flip)
     for r in range(top):
-        slots[:, r : r + 1] = (id_cols[:, r : r + 1] * capacity).astype(jnp.float32) + jnp.sum(
-            col_hit[r] * col_rank, axis=1, keepdims=True
-        )
-    scores = logits[...]
-    scores = jnp.exp(scores - jnp.max(scores, axis=1, keepdims=True))
-    route[...] = prob[...] * scores / jnp.sum(scores, axis=1, keepdims=True)
-    raw = filtered[...]
-    stats[q, 0:1] = jnp.sum(raw, axis=0, keepdims=True)
-    stats[q, 1:2] = jnp.sum(raw * raw, axis=0, keepdims=True)
+        flip[r : r + 1] = slot_rows[r]
+    flip[top : 2 * top] = scores
+    slots[...] = jnp.transpose(flip[...])
+
     pl.semaphore_wait(barrier, n_sp - 1 + n_tp - 1)
 
     def spread(at, recv, far_sem, near_sem, s):
@@ -214,34 +266,63 @@
         for j in range(1, n_y):
             share(at, recv, s, behind(j), near_sem.at[s, j], sibling).wait_send()
 
+    @pl.when(e + 1 < n_sp)
+    def _():
+        hand_on().start()
+
+    for j in range(1, n_y):
+        share(act_at, act_recv, 0, q, act_far.at[0, j], far(j)).start()
+    share(act_at, act_recv, 0, q, act_near.at[0, 0], sibling).start()
     for o in range(1, n_tp):
-        tell(o).start()
+        tell_gain(o).start()
+
+    @pl.when(e > 0)
+    def _():
+        hand_on().wait_recv()
+        padded[0:history] = halo_in[...].astype(jnp.float32)
+
+    @pl.when(e == 0)
+    def _():
+        padded[0:history] = jnp.zeros_like(halo_in).astype(jnp.float32)
+
+    convolve(0)
+    stats[q] = jnp.transpose(sums[...])[0:8]
+    for o in range(1, n_tp):
+        tell_head(o).start()
+        tell_stats(o).start()
+    relay(act_at, act_recv, act_near, 0)
     for o in range(1, n_tp):
         t = lax.rem(q + o, n_tp)
-        pltpu.make_async_copy(stats.at[t], stats.at[t], stat_recv.at[t]).wait()
+        heard(stats.at[t], stat_recv, t)
+        heard(gains.at[t], gain_recv, t)
+    channels = proj.shape[0]
     one = stats[0, 0:1]
     two = stats[0, 1:2]
     for t in range(1, n_tp):
         one = one + stats[t, 0:1]
         two = two + stats[t, 1:2]
-    channels = proj.shape[0]
     mean = one / channels
-    var = two / channels - mean * mean
-    normed = (filtered[...] - mean) * lax.rsqrt(var + 1e-05) * gain[...]
-    act[q] = (normed / (1.0 + jnp.exp(-normed))).astype(act.dtype)
-    spread(act_at, act_recv, act_far, act_near, 0)
-    relay(act_at, act_recv, act_near, 0)
+    scale = lax.rsqrt(two / channels - mean * mean + 1e-05)
+    for t in range(n_tp):
+        flip[t : t + 1] = (stats[t, 0:1] / local - mean) * scale
+    flip[n_tp : n_tp + 1] = scale
+    columns[...] = jnp.transpose(flip[...])
+    for o in range(1, n_tp):
+        t = lax.rem(q + o, n_tp)
+        heard(head_at(t), head_recv, t)
     collect(act_at, act_recv, 0)
-    depth = act.shape[1]
-    sums = resid[...].astype(jnp.float32)
-    for t in range(n_tp):
-        sums = sums + lax.dot_general(
-            act[t],
-            proj[t * depth : (t + 1) * depth],
-            (((0,), (0,)), ((), ())),
-            preferred_element_type=jnp.float32,
-        )
-    mixed[...] = sums.astype(mixed.dtype)
+    step = min(64, tokens)
+    for first in range(0, tokens, step):
+        for t in range(n_tp):
+            scaled = act[t, first : first + step].astype(jnp.float32)
+            scaled = scaled * columns[first : first + step, n_tp : n_tp + 1]
+            scaled = (scaled + columns[first : first + step, t : t + 1]) * gains[t]
+            scaled = scaled / (1.0 + jnp.exp(-scaled))
+            normal[first : first + step, t * local : (t + 1) * local] = scaled.astype(normal.dtype)
+    mixed[...] = (
+        resid[...].astype(jnp.float32)
+        + jnp.dot(normal[...], proj[...], preferred_element_type=jnp.float32)
+    ).astype(mixed.dtype)
 
     @pl.loop(0, n_sp)
     def _(k):
@@ -271,7 +352,7 @@
         for r in range(top):
             picks = jnp.where(place == slots[:, r : r + 1], 1.0, 0.0).astype(mixed.dtype)
             got = jnp.dot(picks, returned[x], preferred_element_type=jnp.float32)
-            total[...] += route[:, r : r + 1] * got
+            total[...] += slots[:, top + r : top + r + 1] * got
 
     tile = min(256, ff_local)
     out_tile = min(256, width)
@@ -352,8 +433,14 @@
 
     out[...] = (mixed[...].astype(jnp.float32) + total[...]).astype(out.dtype)
 
+    @pl.when(e + 1 < n_sp)
+    def _():
+        hand_on().wait_send()
+
     for o in range(1, n_tp):
-        tell(o).wait_send()
+        tell_gain(o).wait_send()
+        tell_head(o).wait_send()
+        tell_stats(o).wait_send()
     drain(act_at, act_recv, act_far, act_near, 0)
 
     @pl.loop(0, n_sp)
@@ -367,25 +454,34 @@
         give_back(k).wait_send()
 
 
-def run_layer(filtered, gain, proj, resid, id_rows, id_cols, logits, prob, w_gate, w_up, w_down):
+def run_layer(value, gate, taps, gain, proj, resid, ids, logits, prob, w_gate, w_up, w_down):
     n_sp, n_tp = lax.axis_size("sp"), lax.axis_size("tp")
     n_y = n_tp // 2
     tokens, width = resid.shape
+    local = value.shape[0]
     capacity = 4 * tokens // n_sp
     ff_local = w_gate.shape[2]
+    history = -(-(taps.shape[0] - 1) // 16) * 16
     dma = pltpu.SemaphoreType.DMA
     vmem = pl.BlockSpec(memory_space=pltpu.VMEM)
     return pl.pallas_call(
         functools.partial(expert_kernel, n_sp, n_tp),
         out_shape=jax.ShapeDtypeStruct(resid.shape, resid.dtype),
-        in_specs=[vmem] * 8 + [pl.BlockSpec(memory_space=pl.ANY)] * 3,
+        in_specs=[vmem] * 9 + [pl.BlockSpec(memory_space=pl.ANY)] * 3,
         out_specs=vmem,
         scratch_shapes=[
+            pltpu.VMEM((history + tokens, local), jnp.float32),
+            pltpu.VMEM((tokens, 128), jnp.float32),
+            pltpu.VMEM((history, local), jnp.bfloat16),
+            pltpu.VMEM((history, local), jnp.bfloat16),
+            pltpu.VMEM((n_tp, 1, local), jnp.float32),
             pltpu.VMEM((n_tp, 8, tokens), jnp.float32),
-            pltpu.VMEM((n_tp,) + filtered.shape, jnp.bfloat16),
+            pltpu.VMEM((128, tokens), jnp.float32),
+            pltpu.VMEM((tokens, 128), jnp.float32),
+            pltpu.VMEM((n_tp, tokens, local), jnp.bfloat16),
+            pltpu.VMEM((tokens, local * n_tp), jnp.bfloat16),
             pltpu.VMEM((tokens, width), jnp.bfloat16),
-            pltpu.VMEM((tokens, id_cols.shape[1]), jnp.float32),
-            pltpu.VMEM((tokens, id_cols.shape[1]), jnp.float32),
+            pltpu.VMEM((tokens, 128), jnp.float32),
             pltpu.VMEM((tokens, width), jnp.float32),
             pltpu.VMEM((n_sp, capacity, width), jnp.bfloat16),
             pltpu.VMEM((n_sp, capacity, width * n_tp), jnp.bfloat16),
@@ -397,6 +493,11 @@
             pltpu.VMEM(w_down.shape[1:], jnp.bfloat16),
             dma((3,)),
             dma((2,)),
+            dma((2,)),
+            dma((n_tp,)),
+            dma((n_tp,)),
+            dma((n_tp,)),
+            dma((n_tp,)),
             dma((n_tp,)),
             dma((n_tp,)),
             dma((1, n_tp)),
@@ -415,13 +516,7 @@
         compiler_params=pltpu.CompilerParams(
             collective_id=0, has_side_effects=True, vmem_limit_bytes=52 * 1024 * 1024
         ),
-    )(filtered, gain, proj, resid, id_rows, id_cols, logits, prob, w_gate, w_up, w_down)
-
-
-def from_behind(block, axis, distance):
-    devices = range(lax.axis_size(axis))
-    route = [(i - distance, i) for i in devices if i - distance in devices]
-    return lax.ppermute(block, axis, route)
+    )(value, gate, taps, gain, proj, resid, ids, logits, prob, w_gate, w_up, w_down)
 
 
 def per_device(
@@ -438,27 +533,16 @@
     w_up,
     w_down,
 ):
-    local_tokens = glu_value.shape[1]
-    tap_count = conv_taps.shape[1]
-    gated = (glu_value.astype(jnp.float32) * jax.nn.sigmoid(glu_gate.astype(jnp.float32))).astype(
-        jnp.bfloat16
-    )
-    history = from_behind(gated[:, local_tokens - (tap_count - 1) :], "sp", 1)
-    padded = jnp.concatenate([history, gated], axis=1).astype(jnp.float32)
-    filtered = jnp.zeros(gated.shape, jnp.float32)
-    for offset in range(tap_count):
-        filtered = (
-            filtered + conv_taps[:, offset : offset + 1] * padded[:, offset : offset + local_tokens]
-        )
     return run_layer(
-        filtered,
-        norm_gain[:, None],
+        glu_value,
+        glu_gate,
+        conv_taps.T,
+        norm_gain[None, :],
         out_proj,
         resid,
         expert_ids.T,
-        expert_ids,
-        route_logits,
-        group_prob[:, None],
+        route_logits.T,
+        group_prob[None, :],
         w_gate,
         w_up,
         w_down,

time: 119 us -> 109 us (0.916)
  starting transfers between devices: 4.87 us -> 0 us
  other arithmetic: 4.68 us -> 0 us
  Pallas kernels: 103 us -> 100 us
  local copies, waits for them, and re-layouts: 6.05 us -> 8.16 us
    unnamed x7 -> x19, local copies, waits for them, and re-layouts: 2.34 us -> 8.16 us
    ppermute x1 -> x0, starting transfers between devices: 4.87 us -> none  [from_behind(): return lax.ppermute(block, axis, route)]
    add x1 -> x0, other arithmetic: 3.51 us -> none  [per_device(): filtered + conv_taps[:, offset:offset + 1] * padded[:, offset:offset + lo...]
    pallas_call x1, Pallas kernels: 103 us -> 100 us  [run_layer(): pl.pallas_call(functools.partial(expert_kernel, n_sp, n_tp), out_shape=ja...]
    slice x3 -> x0, local copies, waits for them, and re-layouts: 2.08 us -> none  [the longest x2 2 us: per_device(): conv_taps[:, offset:offset + 1] * padded[:, offset:offset + local_tokens]]
    broadcast_in_dim x2 -> x0, local copies, waits for them, and re-layouts: 1.62 us -> none  [the longest x1 0.81 us: per_device(): group_prob[:, None]]
  transfers between devices with their start and end apart: 1 -> 0, of which waited for: 0 -> 0; matrix products, arithmetic and copies ran while one was open for 4% -> 0% of each run, Pallas kernels for 0% -> 0%
where the time goes in v1:
time: 109 us
  Pallas kernels  100 us (92%)
  local copies, waits for them, and re-layouts  8.16 us (7%)
    pallas_call x1, Pallas kernels, run_layer(): pl.pallas_call(functools.partial(expert_kernel, n_sp, n_tp), out_shape=ja...  100 us
    unnamed x19, local copies, waits for them, and re-layouts  8.16 us

profile of v1, /device:TPU:0, one launch (start us, length us, event | category | flops | bytes accessed | tf_op | source)
XLA Modules:
  0.0 108.6 jit_solution(4491419592241646171)
XLA Ops:
  0.0 0.0 copy-start
  0.0 1.2 %copy-done = bf16[1024,512]{1,0:T(8,128)(2,1)S(1)} copy-done((bf16[1024,512]{1,0:T(8,128)(2,1)S(1)}, bf16[1024,512]{1,0:T(8,128)(2,1)}, u32[]{:S(2)}) %copy-start) | copy-done | bytes 1048600
  1.2 0.0 copy-start.1
  1.2 0.9 copy-done.1
  2.2 0.0 copy-start.2
  2.2 0.9 copy-done.2
  3.1 0.0 copy-start.3
  3.1 0.9 copy-done.3
  4.0 0.0 copy-start.4
  4.0 0.8 copy-done.4
  4.7 0.0 copy-start.5
  4.7 0.7 copy-done.5
  5.4 0.0 copy-start.6
  5.4 0.7 copy-done.6
  6.1 0.0 copy-start.7
  6.1 0.7 copy-done.7
  6.8 0.0 copy-start.8
  6.8 0.7 copy-done.8
  7.5 100.4 %shard_map.118 = bf16[256,512]{1,0:T(8,128)(2,1)S(1)} custom-call(bf16[256,256]{1,0:T(8,128)(2,1)S(1)} %copy-done.2, bf16[256,256]{1,0:T(8,128)(2,1)S(1)} %copy-done.3, f32[31,256]{1,0:T(8,128)S(1)} %bitcast.5, f32[1,256]{1,0:T(1,128)S(1)} %bitcast.8, bf16[1024,512]{1,0:T(8,128)(2,1)S(1)} %copy-done, bf16[256,512]{1,0:T(8,128)(2,1)S(1)} %copy-done.1, ...), custom_call_target="tpu_custom_call" | custom-call | tf_op jit(solution)/shard_map/pallas_call | solution.py:467
  107.9 0.7 copy.14
Async XLA Ops:
  0.0 1.2 %copy-start = (bf16[1024,512]{1,0:T(8,128)(2,1)S(1)}, bf16[1024,512]{1,0:T(8,128)(2,1)}, u32[]{:S(2)}) copy-start(bf16[1024,512]{1,0:T(8,128)(2,1)} %proj.1) | copy-start | bytes 3145732
  1.2 0.9 copy-start.1
  2.2 0.9 copy-start.2
  3.1 0.9 copy-start.3
  4.0 0.8 copy-start.4
  4.7 0.7 copy-start.5
  5.4 0.7 copy-start.6
  6.1 0.7 copy-start.7
  6.8 0.7 copy-start.8

commit v2 on v1

v2 whole, which is shorter than its diff:
```python
import functools

import jax
import jax.numpy as jnp
from jax import lax
from jax.experimental import pallas as pl
from jax.experimental.pallas import tpu as pltpu
from jax.sharding import PartitionSpec as P

MESH = pl.DeviceIdType.MESH


def expert_kernel(
    n_sp,
    n_tp,
    front,
    value_h,
    gate_h,
    taps_h,
    gain_h,
    proj_h,
    resid_h,
    ids_h,
    logits_h,
    prob_h,
    w_gate,
    w_up,
    w_down,
    out,
    value,
    gate,
    taps,
    gain,
    proj,
    resid,
    ids,
    logits,
    prob,
    padded,
    sums,
    halo_out,
    halo_in,
    gains,
    stats,
    stats_head,
    flip,
    columns,
    flip_head,
    columns_head,
    act,
    normal,
    mixed,
    mixed_front,
    picks,
    picks_back,
    weights,
    total,
    outgoing,
    outgoing_front,
    rows,
    hidden,
    results,
    returned,
    gate_v,
    up_v,
    down_v,
    input_sem,
    load_sem,
    halo_sem,
    gain_send,
    gain_recv,
    stat_send,
    stat_recv,
    head_send,
    head_recv,
    last_send,
    last_recv,
    act_recv,
    act_far,
    act_near,
    front_send,
    front_recv,
    whole_send,
    whole_recv,
    part_send,
    part_recv,
    cross_send,
    cross_recv,
    half_send,
    half_recv,
    hid_recv,
    hid_far,
    hid_near,
    ret_send,
    ret_recv,
):
    e = lax.axis_index("sp")
    q = lax.axis_index("tp")
    n_y = n_tp // 2
    y, core = q // 2, q % 2
    sibling = 2 * y + (1 - core)
    _, capacity, width = results.shape
    tokens = mixed.shape[0]
    ff_local = gate_v.shape[1]
    history, local = halo_in.shape
    taken = taps.shape[0]
    top = ids.shape[0]
    middle = history + (tokens - history) // 32 * 16
    pieces = ((history, middle - history), (middle, tokens - middle))
    power = n_sp > 1 and n_sp & (n_sp - 1) == 0
    bits = [e // 2**b % 2 for b in range(n_sp.bit_length() - 1)]

    def source(k):
        if not power:
            return lax.rem(e + k, n_sp)
        if n_sp > 4:
            k = jnp.where(k < 3, lax.rem(2 * k, 3), jnp.where(k == n_sp - 1, 3, k + 1))
        return sum((bits[b] + k // 2**b) % 2 * 2**b for b in range(len(bits)))

    def target(k):
        return source(k) if power else lax.rem(e + n_sp - k, n_sp)

    def far(j):
        return 2 * lax.rem(y + j, n_y) + core

    def above(j):
        return lax.rem(y + j, n_y)

    def below(j):
        return lax.rem(y + n_y - j, n_y)

    def quarter(s, of, first, size):
        at = pl.multiple_of((core * n_y + of) * width + first, min(128, width))
        return rows.at[s, :, pl.ds(at, size)]

    def half(s, c):
        return rows.at[s, :, pl.ds(pl.multiple_of(c * n_y * width, width), n_y * width)]

    def hidden_at(s, t):
        return hidden.at[s, :, pl.ds(pl.multiple_of(t * ff_local, ff_local), ff_local)]

    def remote(src, dst, send, recv, to):
        return pltpu.make_async_remote_copy(
            src_ref=src,
            dst_ref=dst,
            send_sem=send,
            recv_sem=recv,
            device_id=to,
            device_id_type=MESH,
        )

    def arrived(ref, recv):
        pltpu.make_async_copy(ref, ref, recv).wait()

    def tell(o, ref, to, send, recv):
        return remote(ref, to, send.at[o], recv.at[q], (e, lax.rem(q + o, n_tp)))

    def tell_gain(o):
        return tell(o, gain, gains.at[q], gain_send, gain_recv)

    def tell_stats(o):
        return tell(o, stats.at[q], stats.at[q], stat_send, stat_recv)

    def tell_last(o):
        return tell(o, stats_head.at[q], stats_head.at[q], last_send, last_recv)

    def head_at(t):
        return act.at[t, pl.ds(0, history)]

    def tell_head(o):
        return tell(o, head_at(q), head_at(q), head_send, head_recv)

    def hand_on():
        to = (lax.rem(e + 1, n_sp), q)
        return remote(halo_out, halo_in, halo_sem.at[0], halo_sem.at[1], to)

    def piece_at(p, t):
        return act.at[t, pl.ds(pieces[p][0], pieces[p][1])]

    def piece(p, t, send, to):
        return remote(piece_at(p, t), piece_at(p, t), send, act_recv.at[p, t], (e, to))

    def share_front(j):
        ours = mixed.at[:, pl.ds(0, front)]
        return remote(ours, mixed_front.at[y], front_send.at[j], front_recv.at[y], (e, far(j)))

    def dispatch(k):
        to = target(k)
        return remote(
            outgoing.at[to],
            quarter(e, y, 0, width),
            whole_send.at[k],
            whole_recv.at[e],
            (to, q),
        )

    def dispatch_front(k, j):
        to = target(k)
        return remote(
            outgoing_front.at[j - 1, to],
            quarter(e, above(j), 0, front),
            part_send.at[k, j],
            part_recv.at[e, above(j)],
            (to, q),
        )

    def cross(s, j, first):
        ref = quarter(s, y, first, width - first)
        return remote(ref, ref, cross_send.at[s, j], cross_recv.at[s, y], (e, far(j)))

    def halve(s):
        ref = half(s, core)
        return remote(ref, ref, half_send.at[s], half_recv.at[s], (e, sibling))

    def share(s, t, send, to):
        ref = hidden_at(s, t)
        return remote(ref, ref, send, hid_recv.at[s, t], (e, to))

    def give_back(k):
        s = source(k)
        return remote(
            results.at[s], returned.at[e], ret_send.at[k], ret_recv.at[e], (s, q)
        )

    inputs = [
        pltpu.make_async_copy(there, here, input_sem.at[i])
        for i, (there, here) in enumerate(
            (
                (value_h, value),
                (gate_h, gate),
                (taps_h, taps),
                (ids_h, ids),
                (logits_h, logits),
                (prob_h, prob),
                (gain_h, gain),
                (proj_h, proj),
                (resid_h, resid),
            )
        )
    ]
    loads = []
    for i, (there, here) in enumerate(((w_gate, gate_v), (w_up, up_v))):
        for t in range(n_tp):
            at = (t % 2 * n_y + t // 2) * width
            loads.append(
                pltpu.make_async_copy(
                    there.at[0, pl.ds(t * width, width)],
                    here.at[pl.ds(at, width)],
                    load_sem.at[i * n_tp + t],
                )
            )
    loads.append(pltpu.make_async_copy(w_down.at[0], down_v, load_sem.at[2 * n_tp]))
    for copy in inputs:
        copy.start()
    barrier = pltpu.get_barrier_semaphore()

    @pl.loop(1, n_sp)
    def _(k):
        pl.semaphore_signal(barrier, inc=1, device_id=(source(k), q), device_id_type=MESH)

    for o in range(1, n_tp):
        pl.semaphore_signal(
            barrier, inc=1, device_id=(e, lax.rem(q + o, n_tp)), device_id_type=MESH
        )
    for copy in inputs[:3]:
        copy.wait()
    for load in loads:
        load.start()

    flow = value[...].astype(jnp.float32) / (1.0 + jnp.exp(-gate[...].astype(jnp.float32)))
    flow = jnp.transpose(flow).astype(jnp.bfloat16)
    halo_out[...] = flow[tokens - history :]
    padded[history:] = flow.astype(jnp.float32)
    lane = lax.broadcasted_iota(jnp.int32, (history, 128), 1)

    def convolve(first):
        filtered = jnp.zeros((history, local), jnp.float32)
        for j in range(taken):
            at = first + history - (taken - 1) + j
            filtered = filtered + taps[j : j + 1] * padded[at : at + history]
        one = jnp.sum(filtered, axis=1, keepdims=True)
        two = jnp.sum(filtered * filtered, axis=1, keepdims=True)
        sums[first : first + history] = jnp.where(lane == 0, one, jnp.where(lane == 1, two, 0.0))
        act[q, first : first + history] = (filtered - one / local).astype(act.dtype)

    sums[0:history] = jnp.zeros((history, 128), jnp.float32)
    for first in range(history, tokens, history):
        convolve(first)
    stats[q] = jnp.transpose(sums[...])[0:8]
    for copy in inputs[3:]:
        copy.wait()
    gains[q] = gain[...]
    pl.semaphore_wait(barrier, n_sp - 1 + n_tp - 1)

    @pl.when(e + 1 < n_sp)
    def _():
        hand_on().start()

    for o in range(1, n_tp):
        tell_gain(o).start()
        tell_stats(o).start()
    for p in range(2):
        for j in range(1, n_y):
            piece(p, q, act_far.at[p, j], far(j)).start()
        piece(p, q, act_near.at[p, 0], sibling).start()

    ahead = lax.broadcasted_iota(jnp.int32, (tokens, tokens), 0)
    after = lax.broadcasted_iota(jnp.int32, (tokens, tokens), 1)
    lanes = max(128, n_sp)
    row_no = lax.broadcasted_iota(jnp.int32, (lanes, tokens), 0)
    row_hit = [jnp.where(row_no == ids[r : r + 1], 1.0, 0.0) for r in range(top)]
    row_rank = jnp.dot(
        sum(row_hit).astype(jnp.bfloat16),
        jnp.where(ahead < after, 1.0, 0.0).astype(jnp.bfloat16),
        preferred_element_type=jnp.float32,
    )
    slot_rows = [
        (ids[r : r + 1] * capacity).astype(jnp.float32)
        + jnp.sum(row_hit[r] * row_rank, axis=0, keepdims=True)
        for r in range(top)
    ]
    scores = logits[...]
    scores = jnp.exp(scores - jnp.max(scores, axis=0, keepdims=True))
    scores = prob[...] * scores / jnp.sum(scores, axis=0, keepdims=True)
    weights[...] = jnp.transpose(sum(row_hit[r] * scores[r : r + 1] for r in range(top)))

    @pl.when(e > 0)
    def _():
        hand_on().wait_recv()
        padded[0:history] = halo_in[...].astype(jnp.float32)

    @pl.when(e == 0)
    def _():
        padded[0:history] = jnp.zeros_like(halo_in).astype(jnp.float32)

    convolve(0)
    stats_head[q] = jnp.transpose(jnp.concatenate([sums[0:history]] * (128 // history), axis=0))[0:8]
    for o in range(1, n_tp):
        tell_head(o).start()
        tell_last(o).start()

    @pl.loop(0, n_sp)
    def _(x):
        place = (x * capacity + lax.broadcasted_iota(jnp.int32, (capacity, tokens), 0)).astype(
            jnp.float32
        )
        chosen = jnp.zeros((capacity, tokens), jnp.float32)
        for r in range(top):
            chosen = chosen + jnp.where(place == slot_rows[r], 1.0, 0.0)
        picks[x] = chosen.astype(picks.dtype)
        picks_back[x] = jnp.transpose(chosen).astype(picks.dtype)

    total[...] = jnp.zeros_like(total)
    channels = proj.shape[0]

    def moments(table, into, turned):
        one = table[0, 0:1]
        two = table[0, 1:2]
        for t in range(1, n_tp):
            one = one + table[t, 0:1]
            two = two + table[t, 1:2]
        mean = one / channels
        scale = lax.rsqrt(two / channels - mean * mean + 1e-05)
        into[...] = jnp.zeros_like(into)
        for t in range(n_tp):
            into[t : t + 1] = (table[t, 0:1] / local - mean) * scale
        into[n_tp : n_tp + 1] = scale
        turned[...] = jnp.transpose(into[...])

    def norm(first, size, turned):
        for t in range(n_tp):
            scaled = act[t, first : first + size].astype(jnp.float32)
            scaled = scaled * turned[first : first + size, n_tp : n_tp + 1]
            scaled = (scaled + turned[first : first + size, t : t + 1]) * gains[t]
            scaled = scaled / (1.0 + jnp.exp(-scaled))
            normal[first : first + size, t * local : (t + 1) * local] = scaled.astype(normal.dtype)

    for o in range(1, n_tp):
        t = lax.rem(q + o, n_tp)
        arrived(stats.at[t], stat_recv.at[t])
        arrived(gains.at[t], gain_recv.at[t])
    moments(stats, flip, columns)
    for p in range(2):
        for j in range(1, n_y):
            t = 2 * below(j) + core
            arrived(piece_at(p, t), act_recv.at[p, t])
            piece(p, t, act_near.at[p, j], sibling).start()
    for p in range(2):
        for j in range(n_y):
            t = 2 * below(j) + (1 - core)
            arrived(piece_at(p, t), act_recv.at[p, t])
        first, size = pieces[p]
        step = 56 if size % 56 == 0 else 16
        for at in range(first, first + size, step):
            norm(at, step, columns)
    for o in range(1, n_tp):
        t = lax.rem(q + o, n_tp)
        arrived(stats_head.at[t], last_recv.at[t])
        arrived(head_at(t), head_recv.at[t])
    moments(stats_head, flip_head, columns_head)
    norm(0, history, columns_head)
    mixed[...] = (
        resid[...].astype(jnp.float32)
        + jnp.dot(normal[...], proj[...], preferred_element_type=jnp.float32)
    ).astype(mixed.dtype)

    def pick(x, block):
        got = jnp.dot(picks[x], block, preferred_element_type=jnp.float32)
        return got.astype(outgoing.dtype)

    quarter(e, y, 0, width)[...] = pick(e, mixed[...])
    for j in range(1, n_y):
        cross(e, j, 0).start()
    if front:
        for j in range(1, n_y):
            share_front(j).start()
    near = min(3, n_sp - 1)

    def send(k):
        to = target(k)
        outgoing[to] = pick(to, mixed[...])
        dispatch(k).start()

    def send_front(k):
        to = target(k)
        for j in range(1, n_y):
            outgoing_front[j - 1, to] = pick(to, mixed_front[above(j)])
            dispatch_front(k, j).start()

    pl.loop(1, near)(send)

    def begin(k):
        s = source(k)
        arrived(quarter(s, y, 0, width), whole_recv.at[s])
        for first, chosen in ((0, k < near), (front, k >= near)):

            @pl.when(chosen)
            def _():
                for j in range(1, n_y):
                    cross(s, j, first).start()

    def gather(k):
        s = source(k)
        for first, chosen in ((0, k < near), (front, k >= near)):

            @pl.when(chosen)
            def _():
                for j in range(1, n_y):
                    of = below(j)
                    if first:
                        arrived(quarter(s, of, 0, first), part_recv.at[s, of])
                    arrived(quarter(s, of, first, width - first), cross_recv.at[s, of])

        halve(s).start()

    for j in range(1, n_y):
        arrived(quarter(e, below(j), 0, width), cross_recv.at[e, below(j)])
    halve(e).start()
    send(near)
    begin(1)
    for load in loads:
        load.wait()

    tile = min(256, ff_local)
    out_tile = min(256, width)

    def up_step(s):
        @pl.loop(0, ff_local // tile)
        def _(i):
            at = pl.ds(pl.multiple_of(i * tile, tile), tile)
            g = jnp.dot(rows[s], gate_v[:, at], preferred_element_type=jnp.float32)
            u = jnp.dot(rows[s], up_v[:, at], preferred_element_type=jnp.float32)
            h = (g / (1.0 + jnp.exp(-g)) * u).astype(hidden.dtype)
            hidden[s, :, pl.ds(pl.multiple_of(q * ff_local + i * tile, tile), tile)] = h

    def down_step(s):
        @pl.loop(0, width // out_tile)
        def _(i):
            at = pl.ds(pl.multiple_of(i * out_tile, out_tile), out_tile)
            o = jnp.dot(hidden[s], down_v[:, at], preferred_element_type=jnp.float32)
            results[s, :, at] = o.astype(results.dtype)

    slot_lane = lax.broadcasted_iota(jnp.int32, weights.shape, 1)

    def combine(x, block):
        got = jnp.dot(picks_back[x], block, preferred_element_type=jnp.float32)
        weight = jnp.sum(jnp.where(slot_lane == x, weights[...], 0.0), axis=1, keepdims=True)
        total[...] += weight * got

    def take(k):
        x = target(k)
        arrived(returned.at[x], ret_recv.at[x])
        combine(x, returned[x])

    def drain(k):
        s = source(k)
        halve(s).wait_send()
        share(s, q, hid_near.at[s, 0], sibling).wait_send()
        for j in range(1, n_y):
            share(s, q, hid_far.at[s, j], far(j)).wait_send()
            share(s, 2 * below(j) + core, hid_near.at[s, j], sibling).wait_send()

        for first, chosen in ((0, k < near), (front, k >= near)):

            @pl.when(chosen)
            def _():
                for j in range(1, n_y):
                    cross(s, j, first).wait_send()
                    if first:
                        dispatch_front(k, j).wait_send()

        @pl.when(k > 0)
        def _():
            dispatch(k).wait_send()

    @pl.loop(2, n_sp + 4)
    def _(i):
        @pl.when(i < n_sp + 2)
        def _():
            s = source(i - 2)
            arrived(half(s, 1 - core), half_recv.at[s])
            up_step(s)
            for j in range(1, n_y):
                share(s, q, hid_far.at[s, j], far(j)).start()
            share(s, q, hid_near.at[s, 0], sibling).start()

        if front:

            @pl.when(i == 2)
            def _():
                for j in range(1, n_y):
                    arrived(mixed_front.at[below(j)], front_recv.at[below(j)])

            @pl.when(i - 2 + near < n_sp)
            def _():
                send_front(i - 2 + near)

        @pl.when(i - 1 + near < n_sp)
        def _():
            send(i - 1 + near)

        @pl.when(i < n_sp)
        def _():
            begin(i)

        @pl.when(i < n_sp + 1)
        def _():
            gather(i - 1)

        @pl.when((i >= 3) & (i < n_sp + 3))
        def _():
            s = source(i - 3)
            for j in range(1, n_y):
                t = 2 * below(j) + core
                arrived(hidden_at(s, t), hid_recv.at[s, t])
                share(s, t, hid_near.at[s, j], sibling).start()

        @pl.when(i >= 4)
        def _():
            s = source(i - 4)
            for j in range(n_y):
                t = 2 * below(j) + (1 - core)
                arrived(hidden_at(s, t), hid_recv.at[s, t])
            down_step(s)

            @pl.when(i == 4)
            def _():
                combine(e, results[e])

            @pl.when(i > 4)
            def _():
                give_back(i - 4).start()

        @pl.when(i >= 5)
        def _():
            drain(i - 5)

        @pl.when(i >= 8)
        def _():
            take(i - 7)

    for k in range(max(1, n_sp - 3), n_sp):
        take(k)
    out[...] = (mixed[...].astype(jnp.float32) + total[...]).astype(out.dtype)

    drain(n_sp - 1)

    @pl.loop(1, n_sp)
    def _(k):
        give_back(k).wait_send()

    @pl.when(e + 1 < n_sp)
    def _():
        hand_on().wait_send()

    for o in range(1, n_tp):
        tell_gain(o).wait_send()
        tell_stats(o).wait_send()
        tell_head(o).wait_send()
        tell_last(o).wait_send()
    for p in range(2):
        piece(p, q, act_near.at[p, 0], sibling).wait_send()
        for j in range(1, n_y):
            piece(p, q, act_far.at[p, j], far(j)).wait_send()
            piece(p, 2 * below(j) + core, act_near.at[p, j], sibling).wait_send()
    if front:
        for j in range(1, n_y):
            share_front(j).wait_send()


def run_layer(value, gate, taps, gain, proj, resid, ids, logits, prob, w_gate, w_up, w_down):
    n_sp, n_tp = lax.axis_size("sp"), lax.axis_size("tp")
    n_y = n_tp // 2
    tokens, width = resid.shape
    local = value.shape[0]
    capacity = 4 * tokens // n_sp
    ff_local = w_gate.shape[2]
    history = -(-(taps.shape[0] - 1) // 16) * 16
    front = width // 256 * 128
    span = max(front, 128)
    lanes = max(128, n_sp)
    dma = pltpu.SemaphoreType.DMA
    small = (value, gate, taps, gain, proj, resid, ids, logits, prob)
    return pl.pallas_call(
        functools.partial(expert_kernel, n_sp, n_tp, front),
        out_shape=pltpu.VMEM(resid.shape, resid.dtype),
        in_specs=[pl.BlockSpec(memory_space=pltpu.HBM)] * 12,
        out_specs=pl.BlockSpec(memory_space=pltpu.VMEM),
        scratch_shapes=[pltpu.VMEM(x.shape, x.dtype) for x in small]
        + [
            pltpu.VMEM((history + tokens, local), jnp.float32),
            pltpu.VMEM((tokens, 128), jnp.float32),
            pltpu.VMEM((history, local), jnp.bfloat16),
            pltpu.VMEM((history, local), jnp.bfloat16),
            pltpu.VMEM((n_tp, 1, local), jnp.float32),
            pltpu.VMEM((n_tp, 8, tokens), jnp.float32),
            pltpu.VMEM((n_tp, 8, 128), jnp.float32),
            pltpu.VMEM((128, tokens), jnp.float32),
            pltpu.VMEM((tokens, 128), jnp.float32),
            pltpu.VMEM((128, 128), jnp.float32),
            pltpu.VMEM((128, 128), jnp.float32),
            pltpu.VMEM((n_tp, tokens, local), jnp.bfloat16),
            pltpu.VMEM((tokens, local * n_tp), jnp.bfloat16),
            pltpu.VMEM((tokens, width), jnp.bfloat16),
            pltpu.VMEM((n_y, tokens, span), jnp.bfloat16),
            pltpu.VMEM((n_sp, capacity, tokens), jnp.bfloat16),
            pltpu.VMEM((n_sp, tokens, capacity), jnp.bfloat16),
            pltpu.VMEM((tokens, lanes), jnp.float32),
            pltpu.VMEM((tokens, width), jnp.float32),
            pltpu.VMEM((n_sp, capacity, width), jnp.bfloat16),
            pltpu.VMEM((n_y - 1 if front else 1, n_sp, capacity, span), jnp.bfloat16),
            pltpu.VMEM((n_sp, capacity, width * n_tp), jnp.bfloat16),
            pltpu.VMEM((n_sp, capacity, ff_local * n_tp), jnp.bfloat16),
            pltpu.VMEM((n_sp, capacity, width), jnp.bfloat16),
            pltpu.VMEM((n_sp, capacity, width), jnp.bfloat16),
            pltpu.VMEM(w_gate.shape[1:], jnp.bfloat16),
            pltpu.VMEM(w_up.shape[1:], jnp.bfloat16),
            pltpu.VMEM(w_down.shape[1:], jnp.bfloat16),
            dma((len(small),)),
            dma((2 * n_tp + 1,)),
            dma((2,)),
        ]
        + [dma((n_tp,))] * 8
        + [
            dma((2, n_tp)),
            dma((2, n_y)),
            dma((2, n_y)),
            dma((n_y,)),
            dma((n_y,)),
            dma((n_sp,)),
            dma((n_sp,)),
            dma((n_sp, n_y)),
            dma((n_sp, n_y)),
            dma((n_sp, n_y)),
            dma((n_sp, n_y)),
            dma((n_sp,)),
            dma((n_sp,)),
            dma((n_sp, n_tp)),
            dma((n_sp, n_y)),
            dma((n_sp, n_y)),
            dma((n_sp,)),
            dma((n_sp,)),
        ],
        compiler_params=pltpu.CompilerParams(
            collective_id=0, has_side_effects=True, vmem_limit_bytes=57000000
        ),
    )(*small, w_gate, w_up, w_down)


def per_device(
    glu_value,
    glu_gate,
    conv_taps,
    norm_gain,
    out_proj,
    resid,
    expert_ids,
    route_logits,
    group_prob,
    w_gate,
    w_up,
    w_down,
):
    return run_layer(
        glu_value,
        glu_gate,
        conv_taps.T,
        norm_gain[None, :],
        out_proj,
        resid,
        expert_ids.T,
        route_logits.T,
        group_prob[None, :],
        w_gate,
        w_up,
        w_down,
    )


def solution(mesh):
    return jax.shard_map(
        per_device,
        mesh=mesh,
        in_specs=(
            P("tp", "sp"),
            P("tp", "sp"),
            P("tp", None),
            P("tp"),
            P(None, "tp"),
            P("sp", "tp"),
            P("sp", None),
            P("sp", None),
            P("sp"),
            P("sp", None, "tp"),
            P("sp", None, "tp"),
            P("sp", None, "tp"),
        ),
        out_specs=P("sp", "tp"),
        check_vma=False,
    )
```

time: 109 us -> 92.2 us (0.85)
  Pallas kernels: 100 us -> 91.4 us
  local copies, waits for them, and re-layouts: 8.16 us -> 0.71 us
    pallas_call x1, Pallas kernels: 100 us -> 91.4 us  [run_layer(): pl.pallas_call(functools.partial(expert_kernel, n_sp, n_tp, front), out_s...]
    unnamed x19 -> x1, local copies, waits for them, and re-layouts: 8.16 us -> 0.71 us
where the time goes in v2:
time: 92.2 us; the launch traced here: 92.1 us
  Pallas kernels  91.4 us (99%)
    pallas_call x1, Pallas kernels, run_layer(): pl.pallas_call(functools.partial(expert_kernel, n_sp, n_tp, front), out_s...  91.4 us

profile of v2, /device:TPU:0, one launch (start us, length us, event | category | flops | bytes accessed | tf_op | source)
XLA Modules:
  0.0 92.1 jit_solution(16405320717060170852)
XLA Ops:
  0.0 91.4 %shard_map.118 = bf16[256,512]{1,0:T(8,128)(2,1)S(1)} custom-call(bf16[256,256]{1,0:T(8,128)(2,1)} %value_h.1, bf16[256,256]{1,0:T(8,128)(2,1)} %gate_h.1, f32[31,256]{1,0:T(8,128)} %bitcast.5, f32[1,256]{1,0:T(1,128)} %bitcast.8, bf16[1024,512]{1,0:T(8,128)(2,1)} %proj_h.1, bf16[256,512]{1,0:T(8,128)(2,1)} %resid_h.1, s32[2,256]{1,0:T(2,128)} %bitcast.6, ...), custom_call_target="tpu_custom_call" | custom-call | tf_op jit(solution)/shard_map/pallas_call | solution.py:624
  91.4 0.7 copy.14

commit v3 on v2

--- a/solution.py
+++ b/solution.py
@@ -51,7 +51,12 @@
     normal,
     mixed,
     mixed_front,
+    slots,
+    slots_far,
+    tok,
+    tok_front,
     picks,
+    picks_far,
     picks_back,
     weights,
     total,
@@ -80,6 +85,10 @@
     act_near,
     front_send,
     front_recv,
+    slot_sem,
+    tok_sem,
+    tok_send,
+    tok_recv,
     whole_send,
     whole_recv,
     part_send,
@@ -102,23 +111,26 @@
     _, capacity, width = results.shape
     tokens = mixed.shape[0]
     ff_local = gate_v.shape[1]
+    parts = hid_recv.shape[2]
+    ff_part = ff_local // parts
     history, local = halo_in.shape
     taken = taps.shape[0]
     top = ids.shape[0]
     middle = history + (tokens - history) // 32 * 16
     pieces = ((history, middle - history), (middle, tokens - middle))
-    power = n_sp > 1 and n_sp & (n_sp - 1) == 0
+    far_by = n_sp // 2
     bits = [e // 2**b % 2 for b in range(n_sp.bit_length() - 1)]
 
+    def moved(v):
+        return sum((bits[b] + v // 2**b) % 2 * 2**b for b in range(len(bits)))
+
+    def order(k):
+        return lax.rem(k + 1, n_sp)
+
     def source(k):
-        if not power:
-            return lax.rem(e + k, n_sp)
-        if n_sp > 4:
-            k = jnp.where(k < 3, lax.rem(2 * k, 3), jnp.where(k == n_sp - 1, 3, k + 1))
-        return sum((bits[b] + k // 2**b) % 2 * 2**b for b in range(len(bits)))
-
-    def target(k):
-        return source(k) if power else lax.rem(e + n_sp - k, n_sp)
+        return moved(order(k))
+
+    partner = moved(far_by)
 
     def far(j):
         return 2 * lax.rem(y + j, n_y) + core
@@ -136,8 +148,9 @@
     def half(s, c):
         return rows.at[s, :, pl.ds(pl.multiple_of(c * n_y * width, width), n_y * width)]
 
-    def hidden_at(s, t):
-        return hidden.at[s, :, pl.ds(pl.multiple_of(t * ff_local, ff_local), ff_local)]
+    def hidden_at(s, t, part):
+        at = pl.multiple_of(t * ff_local + part * ff_part, ff_part)
+        return hidden.at[s, :, pl.ds(at, ff_part)]
 
     def remote(src, dst, send, recv, to):
         return pltpu.make_async_remote_copy(
@@ -184,23 +197,31 @@
         ours = mixed.at[:, pl.ds(0, front)]
         return remote(ours, mixed_front.at[y], front_send.at[j], front_recv.at[y], (e, far(j)))
 
-    def dispatch(k):
-        to = target(k)
+    def share_slots():
+        return remote(slots, slots_far, slot_sem.at[0], slot_sem.at[1], (partner, q))
+
+    def share_tokens():
+        return remote(mixed, tok, tok_sem.at[0], tok_sem.at[1], (partner, q))
+
+    def share_tokens_front(j):
+        of = above(j)
+        ours = mixed_front.at[of]
+        return remote(ours, tok_front.at[of], tok_send.at[of], tok_recv.at[of], (partner, q))
+
+    def dispatch(v, s):
+        to = moved(lax.rem(v, far_by))
         return remote(
-            outgoing.at[to],
-            quarter(e, y, 0, width),
-            whole_send.at[k],
-            whole_recv.at[e],
-            (to, q),
+            outgoing.at[v], quarter(s, y, 0, width), whole_send.at[v], whole_recv.at[s], (to, q)
         )
 
-    def dispatch_front(k, j):
-        to = target(k)
+    def dispatch_front(v, s, j):
+        to = moved(lax.rem(v, far_by))
+        of = above(j)
         return remote(
-            outgoing_front.at[j - 1, to],
-            quarter(e, above(j), 0, front),
-            part_send.at[k, j],
-            part_recv.at[e, above(j)],
+            outgoing_front.at[j - 1, v],
+            quarter(s, of, 0, front),
+            part_send.at[v, j],
+            part_recv.at[s, of],
             (to, q),
         )
 
@@ -212,9 +233,16 @@
         ref = half(s, core)
         return remote(ref, ref, half_send.at[s], half_recv.at[s], (e, sibling))
 
-    def share(s, t, send, to):
-        ref = hidden_at(s, t)
-        return remote(ref, ref, send, hid_recv.at[s, t], (e, to))
+    def share(s, part, j):
+        ref = hidden_at(s, q, part)
+        to = sibling if j == 0 else far(j)
+        send = hid_near.at[s, 0, part] if j == 0 else hid_far.at[s, j, part]
+        return remote(ref, ref, send, hid_recv.at[s, q, part], (e, to))
+
+    def pass_on(s, part, j):
+        t = 2 * below(j) + core
+        ref = hidden_at(s, t, part)
+        return remote(ref, ref, hid_near.at[s, j, part], hid_recv.at[s, t, part], (e, sibling))
 
     def give_back(k):
         s = source(k)
@@ -255,8 +283,8 @@
     barrier = pltpu.get_barrier_semaphore()
 
     @pl.loop(1, n_sp)
-    def _(k):
-        pl.semaphore_signal(barrier, inc=1, device_id=(source(k), q), device_id_type=MESH)
+    def _(v):
+        pl.semaphore_signal(barrier, inc=1, device_id=(moved(v), q), device_id_type=MESH)
 
     for o in range(1, n_tp):
         pl.semaphore_signal(
@@ -319,6 +347,10 @@
         + jnp.sum(row_hit[r] * row_rank, axis=0, keepdims=True)
         for r in range(top)
     ]
+    for r in range(top):
+        slots[r : r + 1] = slot_rows[r]
+    slots[top:] = jnp.zeros((slots.shape[0] - top, tokens), jnp.float32)
+    share_slots().start()
     scores = logits[...]
     scores = jnp.exp(scores - jnp.max(scores, axis=0, keepdims=True))
     scores = prob[...] * scores / jnp.sum(scores, axis=0, keepdims=True)
@@ -408,70 +440,111 @@
         got = jnp.dot(picks[x], block, preferred_element_type=jnp.float32)
         return got.astype(outgoing.dtype)
 
-    quarter(e, y, 0, width)[...] = pick(e, mixed[...])
-    for j in range(1, n_y):
-        cross(e, j, 0).start()
     if front:
         for j in range(1, n_y):
             share_front(j).start()
-    near = min(3, n_sp - 1)
-
-    def send(k):
-        to = target(k)
-        outgoing[to] = pick(to, mixed[...])
-        dispatch(k).start()
-
-    def send_front(k):
-        to = target(k)
+    near = 2
+
+    def send(v):
+        outgoing[v] = pick(moved(v), mixed[...])
+        dispatch(v, e).start()
+
+    def send_front(v):
         for j in range(1, n_y):
-            outgoing_front[j - 1, to] = pick(to, mixed_front[above(j)])
-            dispatch_front(k, j).start()
-
-    pl.loop(1, near)(send)
+            outgoing_front[j - 1, v] = pick(moved(v), mixed_front[above(j)])
+            dispatch_front(v, e, j).start()
+
+    def pick_far(d, block):
+        got = jnp.dot(picks_far[d], block, preferred_element_type=jnp.float32)
+        return got.astype(outgoing.dtype)
+
+    def forward(d):
+        outgoing[far_by + d] = pick_far(d, tok[...])
+        dispatch(far_by + d, partner).start()
+
+    def forward_front(d):
+        for j in range(1, n_y):
+            outgoing_front[j - 1, far_by + d] = pick_far(d, tok_front[above(j)])
+            dispatch_front(far_by + d, partner, j).start()
+
+    pl.loop(1, near + 1)(send)
+    share_tokens().start()
+    pl.loop(near + 1, far_by)(send)
+    quarter(e, y, 0, width)[...] = pick(e, mixed[...])
+    share_slots().wait_recv()
+
+    @pl.loop(0, far_by)
+    def _(d):
+        place = moved(d) * capacity + lax.broadcasted_iota(jnp.int32, (capacity, tokens), 0)
+        chosen = jnp.zeros((capacity, tokens), jnp.float32)
+        for r in range(top):
+            chosen = chosen + jnp.where(place.astype(jnp.float32) == slots_far[r : r + 1], 1.0, 0.0)
+        picks_far[d] = chosen.astype(picks_far.dtype)
+
+    def kinds(k):
+        whole = (k < near) | (k == n_sp - 1) if front else k < n_sp
+        return ((0, whole), (front, jnp.logical_not(whole)))
 
     def begin(k):
         s = source(k)
         arrived(quarter(s, y, 0, width), whole_recv.at[s])
-        for first, chosen in ((0, k < near), (front, k >= near)):
+        for first, chosen in kinds(k):
 
             @pl.when(chosen)
             def _():
-                for j in range(1, n_y):
+                for j in range(1, n_y if first < width else 1):
                     cross(s, j, first).start()
 
     def gather(k):
         s = source(k)
-        for first, chosen in ((0, k < near), (front, k >= near)):
+        for first, chosen in kinds(k):
 
             @pl.when(chosen)
             def _():
                 for j in range(1, n_y):
                     of = below(j)
                     if first:
-                        arrived(quarter(s, of, 0, first), part_recv.at[s, of])
-                    arrived(quarter(s, of, first, width - first), cross_recv.at[s, of])
+
+                        @pl.when(order(k) != far_by)
+                        def _():
+                            arrived(quarter(s, of, 0, first), part_recv.at[s, of])
+
+                    if first < width:
+                        arrived(quarter(s, of, first, width - first), cross_recv.at[s, of])
 
         halve(s).start()
 
+    begin(0)
+    for k in range(1, near):
+        begin(k)
     for j in range(1, n_y):
-        arrived(quarter(e, below(j), 0, width), cross_recv.at[e, below(j)])
-    halve(e).start()
-    send(near)
-    begin(1)
+        cross(e, j, 0).start()
+    if front:
+        for j in range(1, n_y):
+            arrived(mixed_front.at[below(j)], front_recv.at[below(j)])
+        pl.loop(near + 1, far_by)(send_front)
+    gather(0)
     for load in loads:
         load.wait()
 
-    tile = min(256, ff_local)
+    tile = min(256, ff_part)
     out_tile = min(256, width)
 
     def up_step(s):
-        @pl.loop(0, ff_local // tile)
-        def _(i):
-            at = pl.ds(pl.multiple_of(i * tile, tile), tile)
-            g = jnp.dot(rows[s], gate_v[:, at], preferred_element_type=jnp.float32)
-            u = jnp.dot(rows[s], up_v[:, at], preferred_element_type=jnp.float32)
-            h = (g / (1.0 + jnp.exp(-g)) * u).astype(hidden.dtype)
-            hidden[s, :, pl.ds(pl.multiple_of(q * ff_local + i * tile, tile), tile)] = h
+        @pl.loop(0, parts)
+        def _(part):
+            @pl.loop(0, ff_part // tile)
+            def _(i):
+                first = part * ff_part + i * tile
+                at = pl.ds(pl.multiple_of(first, tile), tile)
+                g = jnp.dot(rows[s], gate_v[:, at], preferred_element_type=jnp.float32)
+                u = jnp.dot(rows[s], up_v[:, at], preferred_element_type=jnp.float32)
+                h = (g / (1.0 + jnp.exp(-g)) * u).astype(hidden.dtype)
+                hidden[s, :, pl.ds(pl.multiple_of(q * ff_local + first, tile), tile)] = h
+
+            for j in range(1, n_y):
+                share(s, part, j).start()
+            share(s, part, 0).start()
 
     def down_step(s):
         @pl.loop(0, width // out_tile)
@@ -488,30 +561,36 @@
         total[...] += weight * got
 
     def take(k):
-        x = target(k)
+        x = source(k)
         arrived(returned.at[x], ret_recv.at[x])
         combine(x, returned[x])
 
     def drain(k):
         s = source(k)
         halve(s).wait_send()
-        share(s, q, hid_near.at[s, 0], sibling).wait_send()
-        for j in range(1, n_y):
-            share(s, q, hid_far.at[s, j], far(j)).wait_send()
-            share(s, 2 * below(j) + core, hid_near.at[s, j], sibling).wait_send()
-
-        for first, chosen in ((0, k < near), (front, k >= near)):
+        for part in range(parts):
+            share(s, part, 0).wait_send()
+            for j in range(1, n_y):
+                share(s, part, j).wait_send()
+                pass_on(s, part, j).wait_send()
+
+        v = order(k)
+        for first, chosen in kinds(k):
 
             @pl.when(chosen)
             def _():
-                for j in range(1, n_y):
+                for j in range(1, n_y if first < width else 1):
                     cross(s, j, first).wait_send()
-                    if first:
-                        dispatch_front(k, j).wait_send()
-
-        @pl.when(k > 0)
+                if first:
+
+                    @pl.when(v != far_by)
+                    def _():
+                        for j in range(1, n_y):
+                            dispatch_front(v, s, j).wait_send()
+
+        @pl.when((v != far_by) & (v > 0))
         def _():
-            dispatch(k).wait_send()
+            dispatch(v, s).wait_send()
 
     @pl.loop(2, n_sp + 4)
     def _(i):
@@ -520,28 +599,46 @@
             s = source(i - 2)
             arrived(half(s, 1 - core), half_recv.at[s])
             up_step(s)
-            for j in range(1, n_y):
-                share(s, q, hid_far.at[s, j], far(j)).start()
-            share(s, q, hid_near.at[s, 0], sibling).start()
+
+        @pl.when(i == 3)
+        def _():
+            arrived(tok, tok_sem.at[1])
+            quarter(partner, y, 0, width)[...] = pick_far(0, tok[...])
+            for j in range(1, n_y if front < width else 1):
+                cross(partner, j, front).start()
+            pl.loop(1, far_by)(forward)
 
         if front:
 
             @pl.when(i == 2)
             def _():
                 for j in range(1, n_y):
-                    arrived(mixed_front.at[below(j)], front_recv.at[below(j)])
-
-            @pl.when(i - 2 + near < n_sp)
+                    share_tokens_front(j).start()
+
+            @pl.when(i == 4)
             def _():
-                send_front(i - 2 + near)
-
-        @pl.when(i - 1 + near < n_sp)
+                for j in range(1, n_y):
+                    of = below(j)
+                    arrived(tok_front.at[of], tok_recv.at[of])
+                    quarter(partner, of, 0, front)[...] = pick_far(0, tok_front[of])
+                pl.loop(1, far_by)(forward_front)
+
+        @pl.when(i >= 4)
         def _():
-            send(i - 1 + near)
-
-        @pl.when(i < n_sp)
-        def _():
-            begin(i)
+            s = source(i - 4)
+            for part in range(parts):
+                for j in range(n_y):
+                    t = 2 * below(j) + (1 - core)
+                    arrived(hidden_at(s, t, part), hid_recv.at[s, t, part])
+            down_step(s)
+
+            @pl.when(i == n_sp + 3)
+            def _():
+                combine(e, results[e])
+
+            @pl.when(i < n_sp + 3)
+            def _():
+                give_back(i - 4).start()
 
         @pl.when(i < n_sp + 1)
         def _():
@@ -550,42 +647,31 @@
         @pl.when((i >= 3) & (i < n_sp + 3))
         def _():
             s = source(i - 3)
-            for j in range(1, n_y):
-                t = 2 * below(j) + core
-                arrived(hidden_at(s, t), hid_recv.at[s, t])
-                share(s, t, hid_near.at[s, j], sibling).start()
-
-        @pl.when(i >= 4)
+            for part in range(parts):
+                for j in range(1, n_y):
+                    t = 2 * below(j) + core
+                    arrived(hidden_at(s, t, part), hid_recv.at[s, t, part])
+                    pass_on(s, part, j).start()
+
+        @pl.when((i >= near) & (i < n_sp - 1) & (order(i) != far_by))
         def _():
-            s = source(i - 4)
-            for j in range(n_y):
-                t = 2 * below(j) + (1 - core)
-                arrived(hidden_at(s, t), hid_recv.at[s, t])
-            down_step(s)
-
-            @pl.when(i == 4)
-            def _():
-                combine(e, results[e])
-
-            @pl.when(i > 4)
-            def _():
-                give_back(i - 4).start()
+            begin(i)
 
         @pl.when(i >= 5)
         def _():
             drain(i - 5)
 
-        @pl.when(i >= 8)
+        @pl.when(i >= 7)
         def _():
             take(i - 7)
 
-    for k in range(max(1, n_sp - 3), n_sp):
+    for k in range(max(0, n_sp - 3), n_sp - 1):
         take(k)
     out[...] = (mixed[...].astype(jnp.float32) + total[...]).astype(out.dtype)
 
     drain(n_sp - 1)
 
-    @pl.loop(1, n_sp)
+    @pl.loop(0, n_sp - 1)
     def _(k):
         give_back(k).wait_send()
 
@@ -603,9 +689,12 @@
         for j in range(1, n_y):
             piece(p, q, act_far.at[p, j], far(j)).wait_send()
             piece(p, 2 * below(j) + core, act_near.at[p, j], sibling).wait_send()
+    share_slots().wait_send()
+    share_tokens().wait_send()
     if front:
         for j in range(1, n_y):
             share_front(j).wait_send()
+            share_tokens_front(j).wait_send()
 
 
 def run_layer(value, gate, taps, gain, proj, resid, ids, logits, prob, w_gate, w_up, w_down):
@@ -616,8 +705,9 @@
     capacity = 4 * tokens // n_sp
     ff_local = w_gate.shape[2]
     history = -(-(taps.shape[0] - 1) // 16) * 16
-    front = width // 256 * 128
+    front = width
     span = max(front, 128)
+    parts = 2 if ff_local % 512 == 0 else 1
     lanes = max(128, n_sp)
     dma = pltpu.SemaphoreType.DMA
     small = (value, gate, taps, gain, proj, resid, ids, logits, prob)
@@ -643,7 +733,12 @@
             pltpu.VMEM((tokens, local * n_tp), jnp.bfloat16),
             pltpu.VMEM((tokens, width), jnp.bfloat16),
             pltpu.VMEM((n_y, tokens, span), jnp.bfloat16),
+            pltpu.VMEM((8, tokens), jnp.float32),
+            pltpu.VMEM((8, tokens), jnp.float32),
+            pltpu.VMEM((tokens, width), jnp.bfloat16),
+            pltpu.VMEM((n_y, tokens, span), jnp.bfloat16),
             pltpu.VMEM((n_sp, capacity, tokens), jnp.bfloat16),
+            pltpu.VMEM((n_sp // 2, capacity, tokens), jnp.bfloat16),
             pltpu.VMEM((n_sp, tokens, capacity), jnp.bfloat16),
             pltpu.VMEM((tokens, lanes), jnp.float32),
             pltpu.VMEM((tokens, width), jnp.float32),
@@ -667,6 +762,10 @@
             dma((2, n_y)),
             dma((n_y,)),
             dma((n_y,)),
+            dma((2,)),
+            dma((2,)),
+            dma((n_y,)),
+            dma((n_y,)),
             dma((n_sp,)),
             dma((n_sp,)),
             dma((n_sp, n_y)),
@@ -675,9 +774,9 @@
             dma((n_sp, n_y)),
             dma((n_sp,)),
             dma((n_sp,)),
-            dma((n_sp, n_tp)),
-            dma((n_sp, n_y)),
-            dma((n_sp, n_y)),
+            dma((n_sp, n_tp, parts)),
+            dma((n_sp, n_y, parts)),
+            dma((n_sp, n_y, parts)),
             dma((n_sp,)),
             dma((n_sp,)),
         ],

time: 92.2 us -> 81.7 us (0.89)
  Pallas kernels: 91.4 us -> 80.9 us
    pallas_call x1, Pallas kernels: 91.4 us -> 80.9 us  [run_layer(): pl.pallas_call(functools.partial(expert_kernel, n_sp, n_tp, front), out_s...]
where the time goes in v3:
time: 81.7 us; the launch traced here: 81.6 us
  Pallas kernels  80.9 us (99%)
    pallas_call x1, Pallas kernels, run_layer(): pl.pallas_call(functools.partial(expert_kernel, n_sp, n_tp, front), out_s...  80.9 us

profile of v3, /device:TPU:0, one launch (start us, length us, event | category | flops | bytes accessed | tf_op | source)
XLA Modules:
  0.0 81.6 jit_solution(9184451685224144543)
XLA Ops:
  0.0 80.9 %shard_map.118 = bf16[256,512]{1,0:T(8,128)(2,1)S(1)} custom-call(bf16[256,256]{1,0:T(8,128)(2,1)} %value_h.1, bf16[256,256]{1,0:T(8,128)(2,1)} %gate_h.1, f32[31,256]{1,0:T(8,128)} %bitcast.5, f32[1,256]{1,0:T(1,128)} %bitcast.8, bf16[1024,512]{1,0:T(8,128)(2,1)} %proj_h.1, bf16[256,512]{1,0:T(8,128)(2,1)} %resid_h.1, s32[2,256]{1,0:T(2,128)} %bitcast.6, ...), custom_call_target="tpu_custom_call" | custom-call | tf_op jit(solution)/shard_map/pallas_call | solution.py:714
  80.9 0.7 copy.14

commit v4 on v3

--- a/solution.py
+++ b/solution.py
@@ -13,7 +13,6 @@
 def expert_kernel(
     n_sp,
     n_tp,
-    front,
     value_h,
     gate_h,
     taps_h,
@@ -40,7 +39,6 @@
     sums,
     halo_out,
     halo_in,
-    gains,
     stats,
     stats_head,
     flip,
@@ -72,8 +70,6 @@
     input_sem,
     load_sem,
     halo_sem,
-    gain_send,
-    gain_recv,
     stat_send,
     stat_recv,
     head_send,
@@ -81,8 +77,8 @@
     last_send,
     last_recv,
     act_recv,
-    act_far,
-    act_near,
+    act_side,
+    act_send,
     front_send,
     front_recv,
     slot_sem,
@@ -91,15 +87,13 @@
     tok_recv,
     whole_send,
     whole_recv,
-    part_send,
-    part_recv,
     cross_send,
     cross_recv,
     half_send,
     half_recv,
     hid_recv,
-    hid_far,
-    hid_near,
+    hid_side,
+    hid_send,
     ret_send,
     ret_recv,
 ):
@@ -112,6 +106,7 @@
     tokens = mixed.shape[0]
     ff_local = gate_v.shape[1]
     parts = hid_recv.shape[2]
+    near = cross_send.shape[0]
     ff_part = ff_local // parts
     history, local = halo_in.shape
     taken = taps.shape[0]
@@ -165,23 +160,24 @@
     def arrived(ref, recv):
         pltpu.make_async_copy(ref, ref, recv).wait()
 
-    def tell(o, ref, to, send, recv):
-        return remote(ref, to, send.at[o], recv.at[q], (e, lax.rem(q + o, n_tp)))
-
-    def tell_gain(o):
-        return tell(o, gain, gains.at[q], gain_send, gain_recv)
+    def tell(o, ref, send, recv):
+        return remote(ref, ref, send.at[0], recv.at[0], (e, lax.rem(q + o, n_tp)))
 
     def tell_stats(o):
-        return tell(o, stats.at[q], stats.at[q], stat_send, stat_recv)
+        return tell(o, stats.at[q], stat_send, stat_recv)
 
     def tell_last(o):
-        return tell(o, stats_head.at[q], stats_head.at[q], last_send, last_recv)
-
-    def head_at(t):
-        return act.at[t, pl.ds(0, history)]
+        return tell(o, stats_head.at[q], last_send, last_recv)
 
     def tell_head(o):
-        return tell(o, head_at(q), head_at(q), head_send, head_recv)
+        return tell(o, act.at[q, pl.ds(0, history)], head_send, head_recv)
+
+    others = pl.ds(0, n_tp - 1)
+    sent = pl.ds(0, 2 * n_y - 1)
+    all_stats = stats.at[others]
+    all_last = stats_head.at[others]
+    all_heads = act.at[others, pl.ds(0, history)]
+    all_pieces = act.at[sent, pl.ds(history, tokens - history)]
 
     def hand_on():
         to = (lax.rem(e + 1, n_sp), q)
@@ -190,12 +186,20 @@
     def piece_at(p, t):
         return act.at[t, pl.ds(pieces[p][0], pieces[p][1])]
 
-    def piece(p, t, send, to):
-        return remote(piece_at(p, t), piece_at(p, t), send, act_recv.at[p, t], (e, to))
+    def piece(p, j):
+        ref = piece_at(p, q)
+        if j == 0:
+            return remote(ref, ref, act_send.at[0], act_side.at[p], (e, sibling))
+        return remote(ref, ref, act_send.at[0], act_recv.at[p, j - 1], (e, far(j)))
+
+    def pass_piece(p, j):
+        ref = piece_at(p, 2 * below(j) + core)
+        return remote(ref, ref, act_send.at[0], act_side.at[p], (e, sibling))
 
     def share_front(j):
-        ours = mixed.at[:, pl.ds(0, front)]
-        return remote(ours, mixed_front.at[y], front_send.at[j], front_recv.at[y], (e, far(j)))
+        return remote(mixed, mixed_front.at[y], front_send.at[0], front_recv.at[0], (e, far(j)))
+
+    all_fronts = mixed_front.at[pl.ds(0, n_y - 1)]
 
     def share_slots():
         return remote(slots, slots_far, slot_sem.at[0], slot_sem.at[1], (partner, q))
@@ -206,12 +210,18 @@
     def share_tokens_front(j):
         of = above(j)
         ours = mixed_front.at[of]
-        return remote(ours, tok_front.at[of], tok_send.at[of], tok_recv.at[of], (partner, q))
-
-    def dispatch(v, s):
+        return remote(ours, tok_front.at[of], tok_send.at[0], tok_recv.at[0], (partner, q))
+
+    all_tokens = tok_front.at[pl.ds(0, n_y - 1)]
+
+    def dispatch(v, s, kind):
         to = moved(lax.rem(v, far_by))
         return remote(
-            outgoing.at[v], quarter(s, y, 0, width), whole_send.at[v], whole_recv.at[s], (to, q)
+            outgoing.at[v],
+            quarter(s, y, 0, width),
+            whole_send.at[kind],
+            whole_recv.at[s],
+            (to, q),
         )
 
     def dispatch_front(v, s, j):
@@ -219,35 +229,37 @@
         of = above(j)
         return remote(
             outgoing_front.at[j - 1, v],
-            quarter(s, of, 0, front),
-            part_send.at[v, j],
-            part_recv.at[s, of],
+            quarter(s, of, 0, width),
+            whole_send.at[1],
+            whole_recv.at[s],
             (to, q),
         )
 
-    def cross(s, j, first):
-        ref = quarter(s, y, first, width - first)
-        return remote(ref, ref, cross_send.at[s, j], cross_recv.at[s, y], (e, far(j)))
+    def cross(k, j):
+        ref = quarter(source(k), y, 0, width)
+        return remote(ref, ref, cross_send.at[k, j - 1], cross_recv.at[k, j - 1], (e, far(j)))
 
     def halve(s):
         ref = half(s, core)
-        return remote(ref, ref, half_send.at[s], half_recv.at[s], (e, sibling))
+        return remote(ref, ref, half_send.at[0], half_recv.at[s], (e, sibling))
 
     def share(s, part, j):
         ref = hidden_at(s, q, part)
-        to = sibling if j == 0 else far(j)
-        send = hid_near.at[s, 0, part] if j == 0 else hid_far.at[s, j, part]
-        return remote(ref, ref, send, hid_recv.at[s, q, part], (e, to))
+        if j == 0:
+            return remote(ref, ref, hid_send.at[0], hid_side.at[s], (e, sibling))
+        return remote(ref, ref, hid_send.at[0], hid_recv.at[s, j - 1, part], (e, far(j)))
 
     def pass_on(s, part, j):
-        t = 2 * below(j) + core
-        ref = hidden_at(s, t, part)
-        return remote(ref, ref, hid_near.at[s, j, part], hid_recv.at[s, t, part], (e, sibling))
+        ref = hidden_at(s, 2 * below(j) + core, part)
+        return remote(ref, ref, hid_send.at[0], hid_side.at[s], (e, sibling))
+
+    def hidden_bytes(s, blocks):
+        return hidden.at[s, :, pl.ds(0, blocks * ff_local)]
 
     def give_back(k):
         s = source(k)
         return remote(
-            results.at[s], returned.at[e], ret_send.at[k], ret_recv.at[e], (s, q)
+            results.at[s], returned.at[e], ret_send.at[0], ret_recv.at[e], (s, q)
         )
 
     inputs = [
@@ -274,10 +286,10 @@
                 pltpu.make_async_copy(
                     there.at[0, pl.ds(t * width, width)],
                     here.at[pl.ds(at, width)],
-                    load_sem.at[i * n_tp + t],
+                    load_sem.at[i],
                 )
             )
-    loads.append(pltpu.make_async_copy(w_down.at[0], down_v, load_sem.at[2 * n_tp]))
+    loads.append(pltpu.make_async_copy(w_down.at[0], down_v, load_sem.at[2]))
     for copy in inputs:
         copy.start()
     barrier = pltpu.get_barrier_semaphore()
@@ -312,25 +324,26 @@
         act[q, first : first + history] = (filtered - one / local).astype(act.dtype)
 
     sums[0:history] = jnp.zeros((history, 128), jnp.float32)
-    for first in range(history, tokens, history):
+    for first in range(history, middle, history):
         convolve(first)
-    stats[q] = jnp.transpose(sums[...])[0:8]
-    for copy in inputs[3:]:
-        copy.wait()
-    gains[q] = gain[...]
     pl.semaphore_wait(barrier, n_sp - 1 + n_tp - 1)
 
     @pl.when(e + 1 < n_sp)
     def _():
         hand_on().start()
 
+    for j in range(n_y - 1, -1, -1):
+        piece(0, j).start()
+    for first in range(first + history, tokens, history):
+        convolve(first)
+    for copy in inputs[3:]:
+        copy.wait()
+    stats[q, 0:8] = jnp.transpose(sums[...])[0:8]
+    stats[q, 8:9, 0:local] = gain[...]
     for o in range(1, n_tp):
-        tell_gain(o).start()
         tell_stats(o).start()
-    for p in range(2):
-        for j in range(1, n_y):
-            piece(p, q, act_far.at[p, j], far(j)).start()
-        piece(p, q, act_near.at[p, 0], sibling).start()
+    for j in range(n_y - 1, -1, -1):
+        piece(1, j).start()
 
     ahead = lax.broadcasted_iota(jnp.int32, (tokens, tokens), 0)
     after = lax.broadcasted_iota(jnp.int32, (tokens, tokens), 1)
@@ -403,32 +416,24 @@
         for t in range(n_tp):
             scaled = act[t, first : first + size].astype(jnp.float32)
             scaled = scaled * turned[first : first + size, n_tp : n_tp + 1]
-            scaled = (scaled + turned[first : first + size, t : t + 1]) * gains[t]
+            scaled = (scaled + turned[first : first + size, t : t + 1]) * stats[t, 8:9, 0:local]
             scaled = scaled / (1.0 + jnp.exp(-scaled))
             normal[first : first + size, t * local : (t + 1) * local] = scaled.astype(normal.dtype)
 
-    for o in range(1, n_tp):
-        t = lax.rem(q + o, n_tp)
-        arrived(stats.at[t], stat_recv.at[t])
-        arrived(gains.at[t], gain_recv.at[t])
+    arrived(all_stats, stat_recv.at[0])
     moments(stats, flip, columns)
     for p in range(2):
         for j in range(1, n_y):
-            t = 2 * below(j) + core
-            arrived(piece_at(p, t), act_recv.at[p, t])
-            piece(p, t, act_near.at[p, j], sibling).start()
+            arrived(piece_at(p, 2 * below(j) + core), act_recv.at[p, j - 1])
+            pass_piece(p, j).start()
     for p in range(2):
-        for j in range(n_y):
-            t = 2 * below(j) + (1 - core)
-            arrived(piece_at(p, t), act_recv.at[p, t])
         first, size = pieces[p]
+        arrived(act.at[pl.ds(0, n_y), pl.ds(first, size)], act_side.at[p])
         step = 56 if size % 56 == 0 else 16
         for at in range(first, first + size, step):
             norm(at, step, columns)
-    for o in range(1, n_tp):
-        t = lax.rem(q + o, n_tp)
-        arrived(stats_head.at[t], last_recv.at[t])
-        arrived(head_at(t), head_recv.at[t])
+    arrived(all_last, last_recv.at[0])
+    arrived(all_heads, head_recv.at[0])
     moments(stats_head, flip_head, columns_head)
     norm(0, history, columns_head)
     mixed[...] = (
@@ -440,14 +445,12 @@
         got = jnp.dot(picks[x], block, preferred_element_type=jnp.float32)
         return got.astype(outgoing.dtype)
 
-    if front:
-        for j in range(1, n_y):
-            share_front(j).start()
-    near = 2
-
-    def send(v):
+    for j in range(1, n_y):
+        share_front(j).start()
+
+    def send(v, kind):
         outgoing[v] = pick(moved(v), mixed[...])
-        dispatch(v, e).start()
+        dispatch(v, e, kind).start()
 
     def send_front(v):
         for j in range(1, n_y):
@@ -460,16 +463,16 @@
 
     def forward(d):
         outgoing[far_by + d] = pick_far(d, tok[...])
-        dispatch(far_by + d, partner).start()
+        dispatch(far_by + d, partner, 1).start()
 
     def forward_front(d):
         for j in range(1, n_y):
             outgoing_front[j - 1, far_by + d] = pick_far(d, tok_front[above(j)])
             dispatch_front(far_by + d, partner, j).start()
 
-    pl.loop(1, near + 1)(send)
+    pl.loop(1, near + 1)(functools.partial(send, kind=0))
     share_tokens().start()
-    pl.loop(near + 1, far_by)(send)
+    pl.loop(near + 1, far_by)(functools.partial(send, kind=1))
     quarter(e, y, 0, width)[...] = pick(e, mixed[...])
     share_slots().wait_recv()
 
@@ -481,51 +484,39 @@
             chosen = chosen + jnp.where(place.astype(jnp.float32) == slots_far[r : r + 1], 1.0, 0.0)
         picks_far[d] = chosen.astype(picks_far.dtype)
 
-    def kinds(k):
-        whole = (k < near) | (k == n_sp - 1) if front else k < n_sp
-        return ((0, whole), (front, jnp.logical_not(whole)))
-
     def begin(k):
         s = source(k)
         arrived(quarter(s, y, 0, width), whole_recv.at[s])
-        for first, chosen in kinds(k):
-
-            @pl.when(chosen)
-            def _():
-                for j in range(1, n_y if first < width else 1):
-                    cross(s, j, first).start()
+        for j in range(1, n_y):
+            cross(k, j).start()
 
     def gather(k):
         s = source(k)
-        for first, chosen in kinds(k):
-
-            @pl.when(chosen)
-            def _():
-                for j in range(1, n_y):
-                    of = below(j)
-                    if first:
-
-                        @pl.when(order(k) != far_by)
-                        def _():
-                            arrived(quarter(s, of, 0, first), part_recv.at[s, of])
-
-                    if first < width:
-                        arrived(quarter(s, of, first, width - first), cross_recv.at[s, of])
+
+        @pl.when(k < near)
+        def _():
+            for j in range(1, n_y):
+                arrived(quarter(s, below(j), 0, width), cross_recv.at[k, j - 1])
+
+        @pl.when((k >= near) & (s != e) & (s != partner))
+        def _():
+            arrived(half(s, core), whole_recv.at[s])
 
         halve(s).start()
 
-    begin(0)
-    for k in range(1, near):
+    for k in range(near):
         begin(k)
+    arrived(all_fronts, front_recv.at[0])
+    pl.loop(near + 1, far_by)(send_front)
     for j in range(1, n_y):
-        cross(e, j, 0).start()
-    if front:
-        for j in range(1, n_y):
-            arrived(mixed_front.at[below(j)], front_recv.at[below(j)])
-        pl.loop(near + 1, far_by)(send_front)
+        of = below(j)
+        quarter(e, of, 0, width)[...] = pick(e, mixed_front[of])
     gather(0)
-    for load in loads:
-        load.wait()
+    for j in range(1, n_y):
+        share_tokens_front(j).start()
+    arrived(gate_v, load_sem.at[0])
+    arrived(up_v, load_sem.at[1])
+    loads[-1].wait()
 
     tile = min(256, ff_part)
     out_tile = min(256, width)
@@ -565,35 +556,12 @@
         arrived(returned.at[x], ret_recv.at[x])
         combine(x, returned[x])
 
-    def drain(k):
-        s = source(k)
-        halve(s).wait_send()
-        for part in range(parts):
-            share(s, part, 0).wait_send()
-            for j in range(1, n_y):
-                share(s, part, j).wait_send()
-                pass_on(s, part, j).wait_send()
-
-        v = order(k)
-        for first, chosen in kinds(k):
-
-            @pl.when(chosen)
-            def _():
-                for j in range(1, n_y if first < width else 1):
-                    cross(s, j, first).wait_send()
-                if first:
-
-                    @pl.when(v != far_by)
-                    def _():
-                        for j in range(1, n_y):
-                            dispatch_front(v, s, j).wait_send()
-
-        @pl.when((v != far_by) & (v > 0))
-        def _():
-            dispatch(v, s).wait_send()
-
     @pl.loop(2, n_sp + 4)
     def _(i):
+        @pl.when(i == n_sp + 3)
+        def _():
+            take(n_sp - 3)
+
         @pl.when(i < n_sp + 2)
         def _():
             s = source(i - 2)
@@ -604,32 +572,20 @@
         def _():
             arrived(tok, tok_sem.at[1])
             quarter(partner, y, 0, width)[...] = pick_far(0, tok[...])
-            for j in range(1, n_y if front < width else 1):
-                cross(partner, j, front).start()
             pl.loop(1, far_by)(forward)
 
-        if front:
-
-            @pl.when(i == 2)
-            def _():
-                for j in range(1, n_y):
-                    share_tokens_front(j).start()
-
-            @pl.when(i == 4)
-            def _():
-                for j in range(1, n_y):
-                    of = below(j)
-                    arrived(tok_front.at[of], tok_recv.at[of])
-                    quarter(partner, of, 0, front)[...] = pick_far(0, tok_front[of])
-                pl.loop(1, far_by)(forward_front)
+        @pl.when(i == 4)
+        def _():
+            arrived(all_tokens, tok_recv.at[0])
+            for j in range(1, n_y):
+                of = below(j)
+                quarter(partner, of, 0, width)[...] = pick_far(0, tok_front[of])
+            pl.loop(1, far_by)(forward_front)
 
         @pl.when(i >= 4)
         def _():
             s = source(i - 4)
-            for part in range(parts):
-                for j in range(n_y):
-                    t = 2 * below(j) + (1 - core)
-                    arrived(hidden_at(s, t, part), hid_recv.at[s, t, part])
+            arrived(hidden_bytes(s, n_y), hid_side.at[s])
             down_step(s)
 
             @pl.when(i == n_sp + 3)
@@ -650,51 +606,40 @@
             for part in range(parts):
                 for j in range(1, n_y):
                     t = 2 * below(j) + core
-                    arrived(hidden_at(s, t, part), hid_recv.at[s, t, part])
+                    arrived(hidden_at(s, t, part), hid_recv.at[s, j - 1, part])
                     pass_on(s, part, j).start()
 
-        @pl.when((i >= near) & (i < n_sp - 1) & (order(i) != far_by))
-        def _():
-            begin(i)
-
-        @pl.when(i >= 5)
-        def _():
-            drain(i - 5)
-
-        @pl.when(i >= 7)
-        def _():
-            take(i - 7)
-
-    for k in range(max(0, n_sp - 3), n_sp - 1):
+        @pl.when((i >= 6) & (i < n_sp + 3))
+        def _():
+            take(i - 6)
+
+    for k in range(max(0, n_sp - 2), n_sp - 1):
         take(k)
     out[...] = (mixed[...].astype(jnp.float32) + total[...]).astype(out.dtype)
 
-    drain(n_sp - 1)
-
-    @pl.loop(0, n_sp - 1)
-    def _(k):
-        give_back(k).wait_send()
+    every = pl.ds(0, n_sp)
+    for k in range(near):
+        for j in range(1, n_y):
+            cross(k, j).wait_send()
+    arrived(outgoing.at[pl.ds(0, near)], whole_send.at[0])
+    rest = pl.ds(0, n_sp - 2 - near)
+    arrived(rows.at[rest, :, pl.ds(0, n_y * width)], whole_send.at[1])
+    arrived(rows.at[every, :, pl.ds(0, n_y * width)], half_send.at[0])
+    arrived(hidden.at[every, :, pl.ds(0, (2 * n_y - 1) * ff_local)], hid_send.at[0])
+    arrived(results.at[pl.ds(0, n_sp - 1)], ret_send.at[0])
 
     @pl.when(e + 1 < n_sp)
     def _():
         hand_on().wait_send()
 
-    for o in range(1, n_tp):
-        tell_gain(o).wait_send()
-        tell_stats(o).wait_send()
-        tell_head(o).wait_send()
-        tell_last(o).wait_send()
-    for p in range(2):
-        piece(p, q, act_near.at[p, 0], sibling).wait_send()
-        for j in range(1, n_y):
-            piece(p, q, act_far.at[p, j], far(j)).wait_send()
-            piece(p, 2 * below(j) + core, act_near.at[p, j], sibling).wait_send()
+    arrived(all_stats, stat_send.at[0])
+    arrived(all_last, last_send.at[0])
+    arrived(all_heads, head_send.at[0])
+    arrived(all_pieces, act_send.at[0])
     share_slots().wait_send()
     share_tokens().wait_send()
-    if front:
-        for j in range(1, n_y):
-            share_front(j).wait_send()
-            share_tokens_front(j).wait_send()
+    arrived(all_fronts, front_send.at[0])
+    arrived(all_tokens, tok_send.at[0])
 
 
 def run_layer(value, gate, taps, gain, proj, resid, ids, logits, prob, w_gate, w_up, w_down):
@@ -705,14 +650,12 @@
     capacity = 4 * tokens // n_sp
     ff_local = w_gate.shape[2]
     history = -(-(taps.shape[0] - 1) // 16) * 16
-    front = width
-    span = max(front, 128)
     parts = 2 if ff_local % 512 == 0 else 1
     lanes = max(128, n_sp)
     dma = pltpu.SemaphoreType.DMA
     small = (value, gate, taps, gain, proj, resid, ids, logits, prob)
     return pl.pallas_call(
-        functools.partial(expert_kernel, n_sp, n_tp, front),
+        functools.partial(expert_kernel, n_sp, n_tp),
         out_shape=pltpu.VMEM(resid.shape, resid.dtype),
         in_specs=[pl.BlockSpec(memory_space=pltpu.HBM)] * 12,
         out_specs=pl.BlockSpec(memory_space=pltpu.VMEM),
@@ -722,8 +665,7 @@
             pltpu.VMEM((tokens, 128), jnp.float32),
             pltpu.VMEM((history, local), jnp.bfloat16),
             pltpu.VMEM((history, local), jnp.bfloat16),
-            pltpu.VMEM((n_tp, 1, local), jnp.float32),
-            pltpu.VMEM((n_tp, 8, tokens), jnp.float32),
+            pltpu.VMEM((n_tp, 16, tokens), jnp.float32),
             pltpu.VMEM((n_tp, 8, 128), jnp.float32),
             pltpu.VMEM((128, tokens), jnp.float32),
             pltpu.VMEM((tokens, 128), jnp.float32),
@@ -732,18 +674,18 @@
             pltpu.VMEM((n_tp, tokens, local), jnp.bfloat16),
             pltpu.VMEM((tokens, local * n_tp), jnp.bfloat16),
             pltpu.VMEM((tokens, width), jnp.bfloat16),
-            pltpu.VMEM((n_y, tokens, span), jnp.bfloat16),
+            pltpu.VMEM((n_y, tokens, width), jnp.bfloat16),
             pltpu.VMEM((8, tokens), jnp.float32),
             pltpu.VMEM((8, tokens), jnp.float32),
             pltpu.VMEM((tokens, width), jnp.bfloat16),
-            pltpu.VMEM((n_y, tokens, span), jnp.bfloat16),
+            pltpu.VMEM((n_y, tokens, width), jnp.bfloat16),
             pltpu.VMEM((n_sp, capacity, tokens), jnp.bfloat16),
             pltpu.VMEM((n_sp // 2, capacity, tokens), jnp.bfloat16),
             pltpu.VMEM((n_sp, tokens, capacity), jnp.bfloat16),
             pltpu.VMEM((tokens, lanes), jnp.float32),
             pltpu.VMEM((tokens, width), jnp.float32),
             pltpu.VMEM((n_sp, capacity, width), jnp.bfloat16),
-            pltpu.VMEM((n_y - 1 if front else 1, n_sp, capacity, span), jnp.bfloat16),
+            pltpu.VMEM((n_y - 1, n_sp, capacity, width), jnp.bfloat16),
             pltpu.VMEM((n_sp, capacity, width * n_tp), jnp.bfloat16),
             pltpu.VMEM((n_sp, capacity, ff_local * n_tp), jnp.bfloat16),
             pltpu.VMEM((n_sp, capacity, width), jnp.bfloat16),
@@ -752,32 +694,30 @@
             pltpu.VMEM(w_up.shape[1:], jnp.bfloat16),
             pltpu.VMEM(w_down.shape[1:], jnp.bfloat16),
             dma((len(small),)),
-            dma((2 * n_tp + 1,)),
+            dma((3,)),
             dma((2,)),
         ]
-        + [dma((n_tp,))] * 8
+        + [dma((1,))] * 6
         + [
-            dma((2, n_tp)),
-            dma((2, n_y)),
-            dma((2, n_y)),
-            dma((n_y,)),
-            dma((n_y,)),
+            dma((2, n_y - 1)),
+            dma((2,)),
+            dma((1,)),
+            dma((1,)),
+            dma((1,)),
             dma((2,)),
             dma((2,)),
-            dma((n_y,)),
-            dma((n_y,)),
+            dma((1,)),
+            dma((1,)),
+            dma((2,)),
             dma((n_sp,)),
+            dma((2, n_y - 1)),
+            dma((2, n_y - 1)),
+            dma((1,)),
             dma((n_sp,)),
-            dma((n_sp, n_y)),
-            dma((n_sp, n_y)),
-            dma((n_sp, n_y)),
-            dma((n_sp, n_y)),
+            dma((n_sp, n_y - 1, parts)),
             dma((n_sp,)),
-            dma((n_sp,)),
-            dma((n_sp, n_tp, parts)),
-            dma((n_sp, n_y, parts)),
-            dma((n_sp, n_y, parts)),
-            dma((n_sp,)),
+            dma((1,)),
+            dma((1,)),
             dma((n_sp,)),
         ],
         compiler_params=pltpu.CompilerParams(

time: 81.7 us -> 78.3 us (0.958)
  Pallas kernels: 80.9 us -> 76.8 us
    pallas_call x1, Pallas kernels: 80.9 us -> 76.8 us  [run_layer(): pl.pallas_call(functools.partial(expert_kernel, n_sp, n_tp), out_shape=pl...]
where the time goes in v4:
time: 78.3 us; the launch traced here: 77.6 us
  Pallas kernels  76.8 us (98%)
    pallas_call x1, Pallas kernels, run_layer(): pl.pallas_call(functools.partial(expert_kernel, n_sp, n_tp), out_shape=pl...  76.8 us

profile of v4, /device:TPU:0, one launch (start us, length us, event | category | flops | bytes accessed | tf_op | source)
XLA Modules:
  0.0 77.6 jit_solution(15481429210946430513)
XLA Ops:
  0.0 76.8 %shard_map.118 = bf16[256,512]{1,0:T(8,128)(2,1)S(1)} custom-call(bf16[256,256]{1,0:T(8,128)(2,1)} %value_h.1, bf16[256,256]{1,0:T(8,128)(2,1)} %gate_h.1, f32[31,256]{1,0:T(8,128)} %bitcast.5, f32[1,256]{1,0:T(1,128)} %bitcast.8, bf16[1024,512]{1,0:T(8,128)(2,1)} %proj_h.1, bf16[256,512]{1,0:T(8,128)(2,1)} %resid_h.1, s32[2,256]{1,0:T(2,128)} %bitcast.6, ...), custom_call_target="tpu_custom_call" | custom-call | tf_op jit(solution)/shard_map/pallas_call | solution.py:657
  76.8 0.7 copy.14

commit v5 on v4

--- a/solution.py
+++ b/solution.py
@@ -256,11 +256,9 @@
     def hidden_bytes(s, blocks):
         return hidden.at[s, :, pl.ds(0, blocks * ff_local)]
 
-    def give_back(k):
-        s = source(k)
-        return remote(
-            results.at[s], returned.at[e], ret_send.at[0], ret_recv.at[e], (s, q)
-        )
+    def give_back(s, at):
+        here, there = results.at[s, :, at], returned.at[e, :, at]
+        return remote(here, there, ret_send.at[0], ret_recv.at[e], (s, q))
 
     inputs = [
         pltpu.make_async_copy(there, here, input_sem.at[i])
@@ -338,8 +336,8 @@
         convolve(first)
     for copy in inputs[3:]:
         copy.wait()
-    stats[q, 0:8] = jnp.transpose(sums[...])[0:8]
-    stats[q, 8:9, 0:local] = gain[...]
+    stats[q] = jnp.transpose(sums[...])[0:8]
+    stats[q, 2:3, 0:local] = gain[...]
     for o in range(1, n_tp):
         tell_stats(o).start()
     for j in range(n_y - 1, -1, -1):
@@ -416,7 +414,7 @@
         for t in range(n_tp):
             scaled = act[t, first : first + size].astype(jnp.float32)
             scaled = scaled * turned[first : first + size, n_tp : n_tp + 1]
-            scaled = (scaled + turned[first : first + size, t : t + 1]) * stats[t, 8:9, 0:local]
+            scaled = (scaled + turned[first : first + size, t : t + 1]) * stats[t, 2:3, 0:local]
             scaled = scaled / (1.0 + jnp.exp(-scaled))
             normal[first : first + size, t * local : (t + 1) * local] = scaled.astype(normal.dtype)
 
@@ -544,6 +542,10 @@
             o = jnp.dot(hidden[s], down_v[:, at], preferred_element_type=jnp.float32)
             results[s, :, at] = o.astype(results.dtype)
 
+            @pl.when(s != e)
+            def _():
+                give_back(s, at).start()
+
     slot_lane = lax.broadcasted_iota(jnp.int32, weights.shape, 1)
 
     def combine(x, block):
@@ -572,7 +574,7 @@
         def _():
             arrived(tok, tok_sem.at[1])
             quarter(partner, y, 0, width)[...] = pick_far(0, tok[...])
-            pl.loop(1, far_by)(forward)
+            pl.loop(1, far_by - 1)(forward)
 
         @pl.when(i == 4)
         def _():
@@ -580,7 +582,12 @@
             for j in range(1, n_y):
                 of = below(j)
                 quarter(partner, of, 0, width)[...] = pick_far(0, tok_front[of])
-            pl.loop(1, far_by)(forward_front)
+            forward(far_by - 1)
+            pl.loop(1, far_by - 1)(forward_front)
+
+        @pl.when(i == 5)
+        def _():
+            forward_front(far_by - 1)
 
         @pl.when(i >= 4)
         def _():
@@ -591,10 +598,6 @@
             @pl.when(i == n_sp + 3)
             def _():
                 combine(e, results[e])
-
-            @pl.when(i < n_sp + 3)
-            def _():
-                give_back(i - 4).start()
 
         @pl.when(i < n_sp + 1)
         def _():
@@ -650,7 +653,7 @@
     capacity = 4 * tokens // n_sp
     ff_local = w_gate.shape[2]
     history = -(-(taps.shape[0] - 1) // 16) * 16
-    parts = 2 if ff_local % 512 == 0 else 1
+    parts = 4 if ff_local % 1024 == 0 else 1
     lanes = max(128, n_sp)
     dma = pltpu.SemaphoreType.DMA
     small = (value, gate, taps, gain, proj, resid, ids, logits, prob)
@@ -665,7 +668,7 @@
             pltpu.VMEM((tokens, 128), jnp.float32),
             pltpu.VMEM((history, local), jnp.bfloat16),
             pltpu.VMEM((history, local), jnp.bfloat16),
-            pltpu.VMEM((n_tp, 16, tokens), jnp.float32),
+            pltpu.VMEM((n_tp, 8, tokens), jnp.float32),
             pltpu.VMEM((n_tp, 8, 128), jnp.float32),
             pltpu.VMEM((128, tokens), jnp.float32),
             pltpu.VMEM((tokens, 128), jnp.float32),

time: 78.3 us -> 77.4 us (0.989)
  Pallas kernels: 76.8 us -> 75.3 us
    pallas_call x1, Pallas kernels: 76.8 us -> 75.3 us  [run_layer(): pl.pallas_call(functools.partial(expert_kernel, n_sp, n_tp), out_shape=pl...]
where the time goes in v5:
time: 77.4 us; the launch traced here: 76 us
  Pallas kernels  75.3 us (97%)
    pallas_call x1, Pallas kernels, run_layer(): pl.pallas_call(functools.partial(expert_kernel, n_sp, n_tp), out_shape=pl...  75.3 us

profile of v5, /device:TPU:0, one launch (start us, length us, event | category | flops | bytes accessed | tf_op | source)
XLA Modules:
  0.0 76.0 jit_solution(14526071395330243717)
XLA Ops:
  0.0 75.3 %shard_map.118 = bf16[256,512]{1,0:T(8,128)(2,1)S(1)} custom-call(bf16[256,256]{1,0:T(8,128)(2,1)} %value_h.1, bf16[256,256]{1,0:T(8,128)(2,1)} %gate_h.1, f32[31,256]{1,0:T(8,128)} %bitcast.5, f32[1,256]{1,0:T(1,128)} %bitcast.8, bf16[1024,512]{1,0:T(8,128)(2,1)} %proj_h.1, bf16[256,512]{1,0:T(8,128)(2,1)} %resid_h.1, s32[2,256]{1,0:T(2,128)} %bitcast.6, ...), custom_call_target="tpu_custom_call" | custom-call | tf_op jit(solution)/shard_map/pallas_call | solution.py:660
  75.3 0.7 copy.14

commit v6 on v5

--- a/solution.py
+++ b/solution.py
@@ -196,8 +196,9 @@
         ref = piece_at(p, 2 * below(j) + core)
         return remote(ref, ref, act_send.at[0], act_side.at[p], (e, sibling))
 
-    def share_front(j):
-        return remote(mixed, mixed_front.at[y], front_send.at[0], front_recv.at[0], (e, far(j)))
+    def share_front(j, at):
+        here, there = mixed.at[:, at], mixed_front.at[y, :, at]
+        return remote(here, there, front_send.at[0], front_recv.at[0], (e, far(j)))
 
     all_fronts = mixed_front.at[pl.ds(0, n_y - 1)]
 
@@ -434,17 +435,18 @@
     arrived(all_heads, head_recv.at[0])
     moments(stats_head, flip_head, columns_head)
     norm(0, history, columns_head)
-    mixed[...] = (
-        resid[...].astype(jnp.float32)
-        + jnp.dot(normal[...], proj[...], preferred_element_type=jnp.float32)
-    ).astype(mixed.dtype)
+    strip = 256 if width % 256 == 0 else width
+    for first in range(0, width, strip):
+        at = pl.ds(first, strip)
+        sums_at = jnp.dot(normal[...], proj[:, at], preferred_element_type=jnp.float32)
+        mixed[:, at] = (resid[:, at].astype(jnp.float32) + sums_at).astype(mixed.dtype)
+        for j in range(1, n_y):
+            share_front(j, at).start()
 
     def pick(x, block):
         got = jnp.dot(picks[x], block, preferred_element_type=jnp.float32)
         return got.astype(outgoing.dtype)
 
-    for j in range(1, n_y):
-        share_front(j).start()
 
     def send(v, kind):
         outgoing[v] = pick(moved(v), mixed[...])

time: 77.4 us -> 77.6 us (level)
  no operation moved by 1% of the time
where the time goes in v6:
time: 77.6 us; the launch traced here: 76.4 us
  Pallas kernels  75.7 us (98%)
    pallas_call x1, Pallas kernels, run_layer(): pl.pallas_call(functools.partial(expert_kernel, n_sp, n_tp), out_shape=pl...  75.7 us

profile of v6, /device:TPU:0, one launch (start us, length us, event | category | flops | bytes accessed | tf_op | source)
XLA Modules:
  0.0 76.4 jit_solution(12425377653934668451)
XLA Ops:
  0.0 75.7 %shard_map.118 = bf16[256,512]{1,0:T(8,128)(2,1)S(1)} custom-call(bf16[256,256]{1,0:T(8,128)(2,1)} %value_h.1, bf16[256,256]{1,0:T(8,128)(2,1)} %gate_h.1, f32[31,256]{1,0:T(8,128)} %bitcast.5, f32[1,256]{1,0:T(1,128)} %bitcast.8, bf16[1024,512]{1,0:T(8,128)(2,1)} %proj_h.1, bf16[256,512]{1,0:T(8,128)(2,1)} %resid_h.1, s32[2,256]{1,0:T(2,128)} %bitcast.6, ...), custom_call_target="tpu_custom_call" | custom-call | tf_op jit(solution)/shard_map/pallas_call | solution.py:662
  75.7 0.7 copy.14
